TPU v7x, 32 devices: a whole 2x2x4 slice. The times are simulated.
32 devices in a mesh: grp: 2 (over y), kv: 4 (over z), tp: 4 (over x, core).
Axes of the slice: x: 2, y: 2, z: 4, core: 2. Of those that a mesh axis runs over, the one named last changes fastest.
Arguments:
- tokens: bfloat16 [48, 4096], P('grp', ('kv', 'tp')), parts along dimension 0, may hold values from -12 to 12
- lengths: int32 [48], P('grp'), parts along dimension 0, may hold values from 1 to 128, 1536 in all
- attn_gain: float32 [4096], P('kv'), may hold values from 0.1 to 1.9
- w_query: bfloat16 [4096, 4096], P('kv', 'tp'), may hold values from -0.09375 to 0.09375
- w_key: bfloat16 [4096, 4096], P('kv', 'tp'), may hold values from -0.09375 to 0.09375
- w_value: bfloat16 [4096, 4096], P('kv', 'tp'), may hold values from -0.09375 to 0.09375
- w_gate: bfloat16 [4096, 4096], P('kv', 'tp'), may hold values from -0.09375 to 0.09375
- log_decay: float32 [16], P('tp'), may hold values from -1 to 0
- key_cache: bfloat16 [48, 128, 4096], P('grp', 'kv', 'tp'), parts along dimension 0, may hold values from -6 to 6
- value_cache: bfloat16 [48, 128, 4096], P('grp', 'kv', 'tp'), parts along dimension 0, may hold values from -6 to 6
- gn_gain: float32 [4096], P('tp'), may hold values from 0.1 to 1.9
- w_out: bfloat16 [4096, 4096], P('tp', 'kv'), may hold values from -0.1875 to 0.1875
- ffn_gain: float32 [4096], P('kv'), may hold values from 0.1 to 1.9
- w_ffn_gate: bfloat16 [4096, 11264], P('kv', 'tp'), may hold values from -0.09375 to 0.09375
- w_ffn_up: bfloat16 [4096, 11264], P('kv', 'tp'), may hold values from -0.09375 to 0.09375
- w_ffn_down: bfloat16 [11264, 4096], P('tp', 'kv'), may hold values from -0.109375 to 0.109375
Outputs:
- layer_out: bfloat16 [48, 4096], P('grp', ('kv', 'tp')), parts along dimension 0
There are 2 independent parts, one for each index of `grp`. A program takes and returns all parts, laid end to end along the dimension named above; an argument that names none is the same for every part. Nothing has to cross between parts.
All inputs are finite; a program needn't handle non-finite values.
Results may differ from a plain program's by a relative error of at most 0.012.
Values may be sent and summed in bfloat16 or wider, within the bound.
A program may use at most 64 MiB of HBM per device.

v0:
```python
import functools
import math

import jax
import jax.numpy as jnp
from jax import lax
from jax.experimental import pallas as pl
from jax.experimental.pallas import tpu as pltpu
from jax.sharding import PartitionSpec as P

DK = 256
D = 4096


RMS_EPS = 0.1
GN_EPS = 1.0
ROPE_BASE = 10000.0


def rotate(vectors, positions):
    half_dim = vectors.shape[-1] // 2
    inverse = ROPE_BASE ** (-jnp.arange(half_dim, dtype=jnp.float32) / half_dim)
    angles = positions[:, None, None] * inverse[None, None, :]
    cosine = jnp.cos(angles)
    sine_part = jnp.sin(angles)
    front_part = vectors[..., :half_dim]
    back_part = vectors[..., half_dim:]
    return jnp.concatenate(
        [front_part * cosine - back_part * sine_part, front_part * sine_part + back_part * cosine],
        axis=-1,
    )


def group_norm(totals, gn_gain):
    width = totals.shape[-1]
    center = jnp.sum(totals, axis=-1, keepdims=True) / width
    spread = jnp.sum(totals * totals, axis=-1, keepdims=True) / width - center * center
    normed = (totals - center) * lax.rsqrt(spread + GN_EPS)
    return normed.reshape(normed.shape[0], -1) * gn_gain


def channel_stat(own_squares):
    return lax.psum(own_squares, "kv")


def input_stat(own_squares):
    return lax.psum(own_squares, "kv")


def cache_partial(query_low, lengths, log_decay, key_cache, value_cache, heads_here):
    batch_rows = query_low.shape[0]
    span = key_cache.shape[1]
    slots = lax.axis_index("kv") * span + jnp.arange(span, dtype=jnp.int32)
    live = slots[None, :] < lengths[:, None]
    gaps = jnp.maximum((lengths[:, None] - slots[None, :]).astype(jnp.float32), 0.0)
    decays = jnp.exp(log_decay[None, None, :] * gaps[:, :, None])
    keys_here = key_cache.reshape(batch_rows, span, heads_here, DK)
    values_here = value_cache.reshape(batch_rows, span, heads_here, DK)
    scores = jnp.einsum("bphd,bhd->bph", keys_here, query_low, preferred_element_type=jnp.float32)
    mixing = jnp.where(live[:, :, None], scores * decays, 0.0).astype(jnp.bfloat16)
    return jnp.einsum("bph,bphd->bhd", mixing, values_here, preferred_element_type=jnp.float32)


def local(
    tokens,
    lengths,
    attn_gain,
    w_query,
    w_key,
    w_value,
    w_gate,
    log_decay,
    key_cache,
    value_cache,
    gn_gain,
    w_out,
    ffn_gain,
    w_ffn_gate,
    w_ffn_up,
    w_ffn_down,
):
    batch_rows = tokens.shape[0]
    heads_here = log_decay.shape[0]
    row_block = lax.all_gather(tokens, "tp", axis=1, tiled=True)
    widened = row_block.astype(jnp.float32)
    own_squares = jnp.sum(widened * widened, axis=1)
    scaled = (widened * attn_gain).astype(jnp.bfloat16)
    part_query = jnp.dot(scaled, w_query, preferred_element_type=jnp.float32)
    part_key = jnp.dot(scaled, w_key, preferred_element_type=jnp.float32)
    part_value = jnp.dot(scaled, w_value, preferred_element_type=jnp.float32)
    part_gate = jnp.dot(scaled, w_gate, preferred_element_type=jnp.float32)
    positions = lengths.astype(jnp.float32)
    total_squares = input_stat(own_squares)
    queries, new_keys, new_values, gates = lax.psum(
        (part_query, part_key, part_value, part_gate), "kv"
    )
    factor = lax.rsqrt(total_squares / D + RMS_EPS)[:, None]
    queries = rotate((queries * factor).reshape(batch_rows, heads_here, DK), positions) * DK ** (
        -0.5
    )
    new_keys = rotate((new_keys * factor).reshape(batch_rows, heads_here, DK), positions)
    new_values = (new_values * factor).reshape(batch_rows, heads_here, DK)
    gates = gates * factor
    query_low = queries.astype(jnp.bfloat16)
    partial_value = cache_partial(query_low, lengths, log_decay, key_cache, value_cache, heads_here)
    cached = lax.psum(partial_value.reshape(batch_rows, heads_here * DK), "kv")
    own_term = jnp.sum(queries * new_keys, axis=-1, keepdims=True) * new_values
    normed = group_norm(cached.reshape(batch_rows, heads_here, DK) + own_term, gn_gain)
    gated = (jax.nn.silu(gates) * normed).astype(jnp.bfloat16)
    out_partial = jnp.dot(gated, w_out, preferred_element_type=jnp.float32)
    mixed = lax.psum_scatter(out_partial, "tp", scatter_dimension=1, tiled=True)
    resid = (tokens.astype(jnp.float32) + mixed).astype(jnp.bfloat16)
    resid_block = lax.all_gather(resid, "tp", axis=1, tiled=True).astype(jnp.float32)
    mid_squares = jnp.sum(resid_block * resid_block, axis=1)
    scaled_mid = (resid_block * ffn_gain).astype(jnp.bfloat16)
    gate_part = jnp.dot(scaled_mid, w_ffn_gate, preferred_element_type=jnp.float32)
    up_part = jnp.dot(scaled_mid, w_ffn_up, preferred_element_type=jnp.float32)
    total_mid = channel_stat(mid_squares)
    gate_sum, up_sum = lax.psum((gate_part, up_part), "kv")
    factor_mid = lax.rsqrt(total_mid / D + RMS_EPS)[:, None]
    hidden = (jax.nn.silu(gate_sum * factor_mid) * (up_sum * factor_mid)).astype(jnp.bfloat16)
    down_partial = jnp.dot(hidden, w_ffn_down, preferred_element_type=jnp.float32)
    down = lax.psum_scatter(down_partial, "tp", scatter_dimension=1, tiled=True)
    return (resid.astype(jnp.float32) + down).astype(jnp.bfloat16)


LANES = 128
F32 = jnp.float32
BF16 = jnp.bfloat16


def window_start(index, tiles, width, parts):
    return (index * (tiles - width) + (parts - 1) // 2) // (parts - 1)


def partner(index, j, parts):
    found, bit = 0, 1
    while bit < parts:
        digit = (index // bit) % 2
        found = found + bit * ((1 - digit) if (j // bit) % 2 else digit)
        bit *= 2
    return found


def pack(value):
    middle = value.shape[1] // 2
    return jnp.concatenate([value[:, :middle], value[:, middle:]], axis=0).astype(BF16)


def unpack(packed):
    wide = packed.astype(F32)
    rows = wide.shape[0] // 2
    return jnp.concatenate([wide[:rows], wide[rows:]], axis=1)


def layer_kernel(
    n_kv,
    n_tp,
    tokens_ref,
    lengths_ref,
    attn_gain_ref,
    log_decay_ref,
    gn_gain_ref,
    ffn_gain_ref,
    wq_hbm,
    wk_hbm,
    wv_hbm,
    wg_hbm,
    kc_hbm,
    vc_hbm,
    wo_hbm,
    wfg_hbm,
    wfu_hbm,
    wfd_hbm,
    out_ref,
    wq,
    wk,
    wv,
    wg,
    kc,
    vc,
    wo,
    wfg,
    wfu,
    wfd,
    tok_buf,
    x_buf,
    sq_send,
    sq_recv,
    q_send,
    q_recv,
    q_full,
    trig,
    decay_buf,
    kvg_send,
    kvg_recv,
    ca_send,
    ca_recv,
    gt_buf,
    o_buf,
    resid_buf,
    sqm_send,
    sqm_recv,
    gu_send,
    gu_recv,
    hid_buf,
    down_buf,
    d_send,
    d_recv,
    load_sem,
    kv_send_sem,
    kv_recv_sem,
    tp_send_sem,
    tp_recv_sem,
):
    rows, own_cols = tokens_ref.shape
    depth, wide = wq.shape
    span = kc.shape[1]
    half = DK // 2
    tiles = wfg.shape[1] // LANES
    win = gu_send.shape[3] * 2
    me_kv = lax.axis_index("kv")
    me_tp = lax.axis_index("tp")

    def kv_peer(j):
        return partner(me_kv, j, n_kv)

    def tp_peer(j):
        return partner(me_tp, j, n_tp)

    kv_order = tuple(range(n_kv - 1, 0, -1))
    tp_order = tuple(range(n_tp - 1, 0, -1))

    loads = {}
    for slot, (name, src, dst) in enumerate(
        (
            ("wq", wq_hbm, wq),
            ("kc", kc_hbm, kc),
            ("vc", vc_hbm, vc),
            ("wk", wk_hbm, wk),
            ("wv", wv_hbm, wv),
            ("wg", wg_hbm, wg),
            ("wo", wo_hbm, wo),
            ("wfg", wfg_hbm, wfg),
            ("wfu", wfu_hbm, wfu),
            ("wfd", wfd_hbm, wfd),
        )
    ):
        loads[name] = pltpu.make_async_copy(src, dst, load_sem.at[slot])

    sent = []

    def to_kv(phase, j, src, dst):
        copy = pltpu.make_async_remote_copy(
            src_ref=src,
            dst_ref=dst,
            send_sem=kv_send_sem.at[phase, j],
            recv_sem=kv_recv_sem.at[phase, j],
            device_id={"kv": kv_peer(j)},
            device_id_type=pl.DeviceIdType.MESH,
        )
        copy.start()
        sent.append(copy)
        return copy

    def to_tp(phase, j, src, dst):
        copy = pltpu.make_async_remote_copy(
            src_ref=src,
            dst_ref=dst,
            send_sem=tp_send_sem.at[phase, j],
            recv_sem=tp_recv_sem.at[phase, j],
            device_id={"tp": tp_peer(j)},
            device_id_type=pl.DeviceIdType.MESH,
        )
        copy.start()
        sent.append(copy)
        return copy

    loads["wq"].start()

    barrier = pltpu.get_barrier_semaphore()
    for j in range(1, n_kv):
        pl.semaphore_signal(
            barrier, inc=1, device_id={"kv": kv_peer(j)}, device_id_type=pl.DeviceIdType.MESH
        )
    for j in range(1, n_tp):
        pl.semaphore_signal(
            barrier, inc=1, device_id={"tp": tp_peer(j)}, device_id_type=pl.DeviceIdType.MESH
        )
    pl.semaphore_wait(barrier, n_kv + n_tp - 2)

    tok_copies = [to_tp(0, j, tokens_ref, tok_buf.at[me_tp]) for j in tp_order]
    for name in ("wk", "wv", "wg", "kc", "vc"):
        loads[name].start()
    tok_buf[me_tp] = tokens_ref[...]

    row_id = lax.broadcasted_iota(jnp.int32, (rows, LANES), 0)
    lens = jnp.zeros((rows, LANES), jnp.int32)
    for b in range(rows):
        lens = jnp.where(row_id == b, lengths_ref[b], lens)
    lane = lax.broadcasted_iota(jnp.int32, (rows, half), 1).astype(F32)
    inverse = jnp.exp(lane * (-math.log(ROPE_BASE) / half))
    angles = lens[:, :1].astype(F32) * inverse
    trig[0] = jnp.cos(angles)
    trig[1] = jnp.sin(angles)
    places = rows * span
    col = lax.broadcasted_iota(jnp.int32, (rows, places), 1)
    row = lax.broadcasted_iota(jnp.int32, (rows, places), 0)
    slot = col - row * span
    position = slot + me_kv * span
    gap = lens[:, :1] - position
    live = (slot >= 0) & (slot < span) & (gap > 0)
    gap_f = jnp.where(live, gap, 0).astype(F32)
    for h in range(n_kv):
        decay_buf[h] = jnp.where(live, jnp.exp(gap_f * log_decay_ref[h]), 0.0)

    def rotate_in(front, back):
        cosine, sine = trig[0], trig[1]
        return front * cosine - back * sine, front * sine + back * cosine

    for copy in tok_copies:
        copy.wait_recv()
    squares = jnp.zeros((rows, 1), F32)
    for c in range(n_tp):
        wide_tok = tok_buf[c].astype(F32)
        squares = squares + jnp.sum(wide_tok * wide_tok, axis=1, keepdims=True)
        cols = pl.ds(c * own_cols, own_cols)
        x_buf[:, cols] = (wide_tok * attn_gain_ref[:, cols]).astype(BF16)
    sq_send[...] = jnp.broadcast_to(squares, (rows, LANES))
    sq_copies = [to_kv(0, j, sq_send, sq_recv.at[j]) for j in kv_order]

    x = x_buf[...]
    loads["wq"].wait()
    q_copies = []
    for part in range(2):
        cols = pl.ds(part * (wide // 2), wide // 2)
        q_own = jnp.dot(x, wq[:, cols], preferred_element_type=F32)
        q_send[part] = pack(q_own)
        q_full[:, cols] = q_own
        for j in kv_order:
            q_copies.append(to_kv(1 + 7 * part, j, q_send.at[part], q_recv.at[part, j]))
    for name in ("wo", "wfg", "wfu", "wfd"):
        loads[name].start()

    for name in ("wk", "wv", "wg"):
        loads[name].wait()
    kvg_copies = []
    for j in kv_order + (0,):
        cols = pl.ds(pl.multiple_of(kv_peer(j) * DK, DK), DK)
        parts = [
            jnp.dot(x, weight[:, cols], preferred_element_type=F32) for weight in (wk, wv, wg)
        ]
        if j:
            kvg_send[j] = pack(jnp.concatenate(parts, axis=1))
            kvg_copies.append(to_kv(2, j, kvg_send.at[j], kvg_recv.at[j]))
        else:
            own_kvg = jnp.concatenate(parts, axis=1)

    for copy in sq_copies:
        copy.wait_recv()
    total_sq = sq_send[...]
    for j in range(1, n_kv):
        total_sq = total_sq + sq_recv[j]
    factor = lax.rsqrt(total_sq / D + RMS_EPS)[:, :1]

    loads["kc"].wait()
    loads["vc"].wait()
    for copy in q_copies:
        copy.wait_recv()
    parts = []
    for part in range(2):
        piece = q_full[:, pl.ds(part * (wide // 2), wide // 2)]
        for j in kv_order:
            piece = piece + unpack(q_recv[part, j])
        parts.append(piece * factor)
    query = jnp.concatenate(parts, axis=1)
    for h in range(n_kv):
        halves = (query[:, h * DK : h * DK + half], query[:, h * DK + half : (h + 1) * DK])
        front, back = rotate_in(*halves)
        q_full[:, pl.ds(h * DK, half)] = front * DK ** (-0.5)
        q_full[:, pl.ds(h * DK + half, half)] = back * DK ** (-0.5)
    ca_copies = []
    for j in kv_order + (0,):
        head = kv_peer(j)
        cols = pl.ds(pl.multiple_of(head * DK, DK), DK)
        keys = kc[:, :, cols].reshape(places, DK)
        scores = lax.dot_general(
            q_full[:, cols].astype(BF16),
            keys,
            (((1,), (1,)), ((), ())),
            preferred_element_type=F32,
        )
        mixing = (scores * decay_buf[head]).astype(BF16)
        values = vc[:, :, cols].reshape(places, DK)
        cached = jnp.dot(mixing, values, preferred_element_type=F32)
        if j:
            ca_send[j] = pack(cached)
            ca_copies.append(to_kv(3, j, ca_send.at[j], ca_recv.at[j]))

    for copy in kvg_copies:
        copy.wait_recv()
    own_head = pl.ds(pl.multiple_of(me_kv * DK, DK), DK)
    for j in kv_order:
        own_kvg = own_kvg + unpack(kvg_recv[j])
    own_kvg = own_kvg * factor
    summed = [own_kvg[:, i * DK : (i + 1) * DK] for i in range(3)]
    new_key, new_value, gate = summed
    front, back = rotate_in(new_key[:, :half], new_key[:, half:])
    query = q_full[:, own_head]
    score = jnp.sum(query[:, :half] * front + query[:, half:] * back, axis=1, keepdims=True)
    own_term = score * new_value
    gate = gate / (1.0 + jnp.exp(-gate))
    totals = own_term + cached
    for copy in ca_copies:
        copy.wait_recv()
    for j in range(1, n_kv):
        totals = totals + unpack(ca_recv[j])
    center = jnp.sum(totals, axis=1, keepdims=True) / DK
    spread = jnp.sum(totals * totals, axis=1, keepdims=True) / DK - center * center
    normed = (totals - center) * lax.rsqrt(spread + GN_EPS) * gn_gain_ref[:, own_head]
    gt_buf[me_kv] = pack(gate * normed)
    gt_copies = [to_kv(4, j, gt_buf.at[me_kv], gt_buf.at[me_kv]) for j in kv_order]

    loads["wo"].wait()
    for copy in gt_copies:
        copy.wait_recv()
    for c in range(n_kv):
        x_buf[:, pl.ds(c * DK, DK)] = unpack(gt_buf[c]).astype(BF16)
    o_buf[me_tp] = pack(jnp.dot(x_buf[...], wo[...], preferred_element_type=F32))
    o_copies = [to_tp(1, j, o_buf.at[me_tp], o_buf.at[me_tp]) for j in tp_order]
    for copy in o_copies:
        copy.wait_recv()
    squares = jnp.zeros((rows, 1), F32)
    mixed = unpack(o_buf[0])
    for t in range(1, n_tp):
        mixed = mixed + unpack(o_buf[t])
    for c in range(n_tp):
        cols = pl.ds(c * own_cols, own_cols)
        own_mixed = mixed[:, c * own_cols : (c + 1) * own_cols]
        resid = (tok_buf[c].astype(F32) + own_mixed).astype(BF16)
        resid_wide = resid.astype(F32)
        resid_buf[c] = resid_wide
        squares = squares + jnp.sum(resid_wide * resid_wide, axis=1, keepdims=True)
        x_buf[:, cols] = (resid_wide * ffn_gain_ref[:, cols]).astype(BF16)
    sqm_send[...] = jnp.broadcast_to(squares, (rows, LANES))
    sqm_copies = [to_kv(5, j, sqm_send, sqm_recv.at[j]) for j in kv_order]

    x = x_buf[...]
    loads["wfg"].wait()
    loads["wfu"].wait()
    gu_copies = []
    for j in kv_order + (0,):
        start = window_start(kv_peer(j), tiles, win // LANES, n_kv)
        cols = pl.ds(pl.multiple_of(start * LANES, LANES), win)
        both = []
        for i, weight in enumerate((wfg, wfu)):
            part = jnp.dot(x, weight[:, cols], preferred_element_type=F32)
            both.append(part)
            if j:
                gu_send[i, j] = pack(part)
                gu_copies.append(to_kv(6 + 3 * i, j, gu_send.at[i, j], gu_recv.at[i, j]))

    for copy in sqm_copies:
        copy.wait_recv()
    total_sq = sqm_send[...]
    for j in range(1, n_kv):
        total_sq = total_sq + sqm_recv[j]
    factor = lax.rsqrt(total_sq / D + RMS_EPS)[:, :1]
    for copy in gu_copies:
        copy.wait_recv()
    for i in range(2):
        for j in kv_order:
            both[i] = both[i] + unpack(gu_recv[i, j])
    gate, up = both[0] * factor, both[1] * factor
    hidden = gate / (1.0 + jnp.exp(-gate)) * up
    here = window_start(me_kv, tiles, win // LANES, n_kv)
    after = window_start(me_kv + 1, tiles, win // LANES, n_kv)
    kept = jnp.where(me_kv == n_kv - 1, win, (after - here) * LANES)
    column = lax.broadcasted_iota(jnp.int32, (rows, win), 1)
    hid_buf[me_kv] = pack(jnp.where(column < kept, hidden, 0.0))
    hid_copies = [to_kv(7, j, hid_buf.at[me_kv], hid_buf.at[me_kv]) for j in kv_order]

    loads["wfd"].wait()
    down = None
    arrivals = dict(zip(kv_order, hid_copies))
    for j in range(n_kv):
        if j:
            arrivals[j].wait_recv()
        source = kv_peer(j)
        start = window_start(source, tiles, win // LANES, n_kv)
        weight = wfd[pl.ds(pl.multiple_of(start * LANES, LANES), win), :]
        chunk = unpack(hid_buf[source]).astype(BF16)
        part = jnp.dot(chunk, weight, preferred_element_type=F32)
        down = part if down is None else down + part
    down_buf[...] = down
    d_copies = {}
    for j in tp_order:
        cols = pl.ds(pl.multiple_of(tp_peer(j) * own_cols, own_cols), own_cols)
        d_send[j] = pack(down_buf[:, cols])
        d_copies[j] = to_tp(2, j, d_send.at[j], d_recv.at[j])
    own = pl.ds(pl.multiple_of(me_tp * own_cols, own_cols), own_cols)
    result = down_buf[:, own] + resid_buf[me_tp]
    for j in range(1, n_tp):
        d_copies[j].wait_recv()
        result = result + unpack(d_recv[j])
    out_ref[...] = result.astype(BF16)
    for copy in sent:
        copy.wait_send()


def fused(
    n_kv,
    n_tp,
    tokens,
    lengths,
    attn_gain,
    w_query,
    w_key,
    w_value,
    w_gate,
    log_decay,
    key_cache,
    value_cache,
    gn_gain,
    w_out,
    ffn_gain,
    w_ffn_gate,
    w_ffn_up,
    w_ffn_down,
):
    rows, own_cols = tokens.shape
    depth, wide = w_query.shape
    units = w_ffn_gate.shape[1]
    tiles = units // LANES
    win = -(-tiles // n_kv // 2) * 2 * LANES
    span = key_cache.shape[1]
    vmem = pl.BlockSpec(memory_space=pltpu.VMEM)
    smem = pl.BlockSpec(memory_space=pltpu.SMEM)
    hbm = pl.BlockSpec(memory_space=pl.ANY)
    streamed = (
        w_query,
        w_key,
        w_value,
        w_gate,
        key_cache,
        value_cache,
        w_out,
        w_ffn_gate,
        w_ffn_up,
        w_ffn_down,
    )
    scratch = [pltpu.VMEM(a.shape, a.dtype) for a in streamed] + [
        pltpu.VMEM((n_tp, rows, own_cols), BF16),
        pltpu.VMEM((rows, depth), BF16),
        pltpu.VMEM((rows, LANES), F32),
        pltpu.VMEM((n_kv, rows, LANES), F32),
        pltpu.VMEM((2, 2 * rows, wide // 4), BF16),
        pltpu.VMEM((2, n_kv, 2 * rows, wide // 4), BF16),
        pltpu.VMEM((rows, wide), F32),
        pltpu.VMEM((2, rows, DK // 2), F32),
        pltpu.VMEM((n_kv, rows, rows * span), F32),
        pltpu.VMEM((n_kv, 2 * rows, 3 * DK // 2), BF16),
        pltpu.VMEM((n_kv, 2 * rows, 3 * DK // 2), BF16),
        pltpu.VMEM((n_kv, 2 * rows, DK // 2), BF16),
        pltpu.VMEM((n_kv, 2 * rows, DK // 2), BF16),
        pltpu.VMEM((n_kv, 2 * rows, DK // 2), BF16),
        pltpu.VMEM((n_tp, 2 * rows, depth // 2), BF16),
        pltpu.VMEM((n_tp, rows, own_cols), F32),
        pltpu.VMEM((rows, LANES), F32),
        pltpu.VMEM((n_kv, rows, LANES), F32),
        pltpu.VMEM((2, n_kv, 2 * rows, win // 2), BF16),
        pltpu.VMEM((2, n_kv, 2 * rows, win // 2), BF16),
        pltpu.VMEM((n_kv, 2 * rows, win // 2), BF16),
        pltpu.VMEM((rows, depth), F32),
        pltpu.VMEM((n_tp, 2 * rows, own_cols // 2), BF16),
        pltpu.VMEM((n_tp, 2 * rows, own_cols // 2), BF16),
        pltpu.SemaphoreType.DMA((len(streamed),)),
        pltpu.SemaphoreType.DMA((10, n_kv)),
        pltpu.SemaphoreType.DMA((10, n_kv)),
        pltpu.SemaphoreType.DMA((3, n_tp)),
        pltpu.SemaphoreType.DMA((3, n_tp)),
    ]
    return pl.pallas_call(
        functools.partial(layer_kernel, n_kv, n_tp),
        out_shape=pltpu.VMEM((rows, own_cols), BF16),
        in_specs=[vmem, smem, vmem, smem, vmem, vmem] + [hbm] * len(streamed),
        out_specs=vmem,
        scratch_shapes=scratch,
        compiler_params=pltpu.CompilerParams(
            collective_id=0, has_side_effects=True, vmem_limit_bytes=60 * 1024 * 1024
        ),
    )(
        tokens,
        lengths,
        attn_gain[None, :],
        log_decay,
        gn_gain[None, :],
        ffn_gain[None, :],
        *streamed,
    )


def fits(mesh, tokens, log_decay, key_cache, w_query, w_ffn_gate):
    n_kv, n_tp, n_grp = mesh.shape["kv"], mesh.shape["tp"], mesh.shape["grp"]
    heads, span = log_decay.shape[0], key_cache.shape[1] // n_kv
    return (
        n_kv > 1
        and n_tp > 1
        and n_kv & (n_kv - 1) == 0
        and n_tp & (n_tp - 1) == 0
        and heads == n_kv * n_tp
        and tokens.shape[1] // n_kv == heads * DK // n_tp
        and tokens.shape[1] % (n_kv * n_tp * 2 * LANES) == 0
        and heads * DK // n_tp % (4 * LANES) == 0
        and w_ffn_gate.shape[1] % (n_tp * LANES) == 0
        and tokens.shape[0] // n_grp % 8 == 0
        and span % 16 == 0
        and span <= 64
    )


def solution(mesh):
    specs = (
        P("grp", ("kv", "tp")),
        P("grp"),
        P("kv"),
        P("kv", "tp"),
        P("kv", "tp"),
        P("kv", "tp"),
        P("kv", "tp"),
        P("tp"),
        P("grp", "kv", "tp"),
        P("grp", "kv", "tp"),
        P("tp"),
        P("tp", "kv"),
        P("kv"),
        P("kv", "tp"),
        P("kv", "tp"),
        P("tp", "kv"),
    )

    def whole(*arrays):
        tokens, w_query, log_decay, key_cache = arrays[0], arrays[3], arrays[7], arrays[8]
        if fits(mesh, tokens, log_decay, key_cache, w_query, arrays[13]):
            body = functools.partial(fused, mesh.shape["kv"], mesh.shape["tp"])
        else:
            body = local
        return jax.shard_map(
            body,
            mesh=mesh,
            in_specs=specs,
            out_specs=P("grp", ("kv", "tp")),
            check_vma=False,
        )(*arrays)

    return whole
```

profile of v0, /device:TPU:0, one launch (start us, length us, event | category | flops | bytes accessed | tf_op | source)
XLA Modules:
  0.0 48.6 jit_solution(8630044649731392750)
XLA Ops:
  0.0 48.0 %shard_map.154 = bf16[24,256]{1,0:T(8,128)(2,1)S(1)} custom-call(bf16[24,256]{1,0:T(8,128)(2,1)} %tokens_ref.1, s32[24]{0:T(128)} %lengths_ref.1, f32[1,1024]{1,0:T(1,128)} %bitcast.3, f32[4]{0:T(128)} %log_decay_ref.1, f32[1,1024]{1,0:T(1,128)} %bitcast.4, f32[1,1024]{1,0:T(1,128)} %bitcast.5, bf16[1024,1024]{1,0:T(8,128)(2,1)} %wq_hbm.1, ...), custom_call_target="tpu_custom_call" | custom-call | tf_op jit(solution)/shard_map/pallas_call | solution.py:583
  48.0 0.6 %copy.18 = bf16[24,256]{1,0:T(8,128)(2,1)} copy(bf16[24,256]{1,0:T(8,128)(2,1)S(1)} %shard_map.154) | data formatting | bytes 24576
where the time goes:
time: 48.8 us; the launch traced here: 48.6 us
  Pallas kernels  48 us (98%)
  local copies, waits for them, and re-layouts  0.6 us (1%)
    pallas_call x1, Pallas kernels, fused(): pl.pallas_call(functools.partial(layer_kernel, n_kv, n_tp), out_shape=plt...  48 us

commit v1 on v0

--- a/solution.py
+++ b/solution.py
@@ -125,6 +125,7 @@
 
 
 LANES = 128
+STAGE_TILES = 2
 F32 = jnp.float32
 BF16 = jnp.bfloat16
 
@@ -153,15 +154,20 @@
     return jnp.concatenate([wide[:rows], wide[rows:]], axis=1)
 
 
+def stage_spans(tiles, n_kv):
+    step = STAGE_TILES * n_kv
+    return [(first, min(step, tiles - first)) for first in range(0, tiles, step)]
+
+
 def layer_kernel(
     n_kv,
     n_tp,
-    tokens_ref,
-    lengths_ref,
-    attn_gain_ref,
-    log_decay_ref,
-    gn_gain_ref,
-    ffn_gain_ref,
+    tokens_hbm,
+    lengths_hbm,
+    attn_gain_hbm,
+    log_decay_hbm,
+    gn_gain_hbm,
+    ffn_gain_hbm,
     wq_hbm,
     wk_hbm,
     wv_hbm,
@@ -183,6 +189,12 @@
     wfg,
     wfu,
     wfd,
+    tokens_ref,
+    lengths_ref,
+    attn_gain_ref,
+    log_decay_ref,
+    gn_gain_ref,
+    ffn_gain_ref,
     tok_buf,
     x_buf,
     sq_send,
@@ -194,13 +206,19 @@
     decay_buf,
     kvg_send,
     kvg_recv,
+    ca_own,
     ca_send,
     ca_recv,
-    gt_buf,
-    o_buf,
+    ot_buf,
+    o_own,
+    o_send,
+    o_recv,
+    chip_send,
+    chip_recv,
     resid_buf,
     sqm_send,
     sqm_recv,
+    gu_own,
     gu_send,
     gu_recv,
     hid_buf,
@@ -218,7 +236,9 @@
     span = kc.shape[1]
     half = DK // 2
     tiles = wfg.shape[1] // LANES
-    win = gu_send.shape[3] * 2
+    win = STAGE_TILES * LANES
+    stages = stage_spans(tiles, n_kv)
+    heads = n_kv
     me_kv = lax.axis_index("kv")
     me_tp = lax.axis_index("tp")
 
@@ -230,10 +250,26 @@
 
     kv_order = tuple(range(n_kv - 1, 0, -1))
     tp_order = tuple(range(n_tp - 1, 0, -1))
+
+    barrier = pltpu.get_barrier_semaphore()
+    for j in range(1, n_kv):
+        pl.semaphore_signal(
+            barrier, inc=1, device_id={"kv": kv_peer(j)}, device_id_type=pl.DeviceIdType.MESH
+        )
+    for j in range(1, n_tp):
+        pl.semaphore_signal(
+            barrier, inc=1, device_id={"tp": tp_peer(j)}, device_id_type=pl.DeviceIdType.MESH
+        )
 
     loads = {}
     for slot, (name, src, dst) in enumerate(
         (
+            ("tok", tokens_hbm, tokens_ref),
+            ("len", lengths_hbm, lengths_ref),
+            ("ag", attn_gain_hbm, attn_gain_ref),
+            ("ld", log_decay_hbm, log_decay_ref),
+            ("gg", gn_gain_hbm, gn_gain_ref),
+            ("fg", ffn_gain_hbm, ffn_gain_ref),
             ("wq", wq_hbm, wq),
             ("kc", kc_hbm, kc),
             ("vc", vc_hbm, vc),
@@ -263,37 +299,37 @@
         sent.append(copy)
         return copy
 
-    def to_tp(phase, j, src, dst):
-        copy = pltpu.make_async_remote_copy(
+    def tp_copy(phase, j, src, dst, slot=None):
+        return pltpu.make_async_remote_copy(
             src_ref=src,
             dst_ref=dst,
             send_sem=tp_send_sem.at[phase, j],
-            recv_sem=tp_recv_sem.at[phase, j],
+            recv_sem=tp_recv_sem.at[phase, j if slot is None else slot],
             device_id={"tp": tp_peer(j)},
             device_id_type=pl.DeviceIdType.MESH,
         )
+
+    def to_tp(phase, j, src, dst):
+        copy = tp_copy(phase, j, src, dst)
         copy.start()
         sent.append(copy)
         return copy
 
-    loads["wq"].start()
-
-    barrier = pltpu.get_barrier_semaphore()
-    for j in range(1, n_kv):
-        pl.semaphore_signal(
-            barrier, inc=1, device_id={"kv": kv_peer(j)}, device_id_type=pl.DeviceIdType.MESH
-        )
-    for j in range(1, n_tp):
-        pl.semaphore_signal(
-            barrier, inc=1, device_id={"tp": tp_peer(j)}, device_id_type=pl.DeviceIdType.MESH
-        )
+    P_SQ, P_Q, P_KVG, P_CA, P_OT = 0, 1, 1 + heads, 2 + heads, 2 + 2 * heads
+    P_SQM, P_GU, P_HID = 3 + 2 * heads, 4 + 2 * heads, 4 + 2 * heads + len(stages)
+
+    for name in ("tok", "len", "ld", "ag", "wq"):
+        loads[name].start()
+    loads["tok"].wait()
     pl.semaphore_wait(barrier, n_kv + n_tp - 2)
 
     tok_copies = [to_tp(0, j, tokens_ref, tok_buf.at[me_tp]) for j in tp_order]
-    for name in ("wk", "wv", "wg", "kc", "vc"):
+    for name in ("wk", "wv", "wg", "kc", "vc", "gg", "fg"):
         loads[name].start()
     tok_buf[me_tp] = tokens_ref[...]
 
+    for name in ("len", "ld", "ag"):
+        loads[name].wait()
     row_id = lax.broadcasted_iota(jnp.int32, (rows, LANES), 0)
     lens = jnp.zeros((rows, LANES), jnp.int32)
     for b in range(rows):
@@ -311,7 +347,7 @@
     gap = lens[:, :1] - position
     live = (slot >= 0) & (slot < span) & (gap > 0)
     gap_f = jnp.where(live, gap, 0).astype(F32)
-    for h in range(n_kv):
+    for h in range(heads):
         decay_buf[h] = jnp.where(live, jnp.exp(gap_f * log_decay_ref[h]), 0.0)
 
     def rotate_in(front, back):
@@ -327,18 +363,20 @@
         cols = pl.ds(c * own_cols, own_cols)
         x_buf[:, cols] = (wide_tok * attn_gain_ref[:, cols]).astype(BF16)
     sq_send[...] = jnp.broadcast_to(squares, (rows, LANES))
-    sq_copies = [to_kv(0, j, sq_send, sq_recv.at[j]) for j in kv_order]
 
     x = x_buf[...]
     loads["wq"].wait()
-    q_copies = []
-    for part in range(2):
-        cols = pl.ds(part * (wide // 2), wide // 2)
+    q_copies = {}
+    sq_copies = None
+    for h in range(heads):
+        cols = pl.ds(h * DK, DK)
         q_own = jnp.dot(x, wq[:, cols], preferred_element_type=F32)
-        q_send[part] = pack(q_own)
+        q_send[h] = pack(q_own)
         q_full[:, cols] = q_own
         for j in kv_order:
-            q_copies.append(to_kv(1 + 7 * part, j, q_send.at[part], q_recv.at[part, j]))
+            q_copies[h, j] = to_kv(P_Q + h, j, q_send.at[h], q_recv.at[h, j])
+        if sq_copies is None:
+            sq_copies = [to_kv(P_SQ, j, sq_send, sq_recv.at[j]) for j in kv_order]
     for name in ("wo", "wfg", "wfu", "wfd"):
         loads[name].start()
 
@@ -352,7 +390,7 @@
         ]
         if j:
             kvg_send[j] = pack(jnp.concatenate(parts, axis=1))
-            kvg_copies.append(to_kv(2, j, kvg_send.at[j], kvg_recv.at[j]))
+            kvg_copies.append(to_kv(P_KVG, j, kvg_send.at[j], kvg_recv.at[j]))
         else:
             own_kvg = jnp.concatenate(parts, axis=1)
 
@@ -365,75 +403,87 @@
 
     loads["kc"].wait()
     loads["vc"].wait()
-    for copy in q_copies:
-        copy.wait_recv()
-    parts = []
-    for part in range(2):
-        piece = q_full[:, pl.ds(part * (wide // 2), wide // 2)]
-        for j in kv_order:
-            piece = piece + unpack(q_recv[part, j])
-        parts.append(piece * factor)
-    query = jnp.concatenate(parts, axis=1)
-    for h in range(n_kv):
-        halves = (query[:, h * DK : h * DK + half], query[:, h * DK + half : (h + 1) * DK])
-        front, back = rotate_in(*halves)
-        q_full[:, pl.ds(h * DK, half)] = front * DK ** (-0.5)
-        q_full[:, pl.ds(h * DK + half, half)] = back * DK ** (-0.5)
-    ca_copies = []
-    for j in kv_order + (0,):
-        head = kv_peer(j)
-        cols = pl.ds(pl.multiple_of(head * DK, DK), DK)
-        keys = kc[:, :, cols].reshape(places, DK)
+    ca_copies = {}
+    for h in range(heads):
+        cols = pl.ds(h * DK, DK)
+        for j in kv_order:
+            q_copies[h, j].wait_recv()
+        query = q_full[:, cols]
+        for j in kv_order:
+            query = query + unpack(q_recv[h, j])
+        query = query * factor
+        front, back = rotate_in(query[:, :half], query[:, half:])
+        query = jnp.concatenate([front, back], axis=1) * DK ** (-0.5)
+        q_full[:, cols] = query
         scores = lax.dot_general(
-            q_full[:, cols].astype(BF16),
-            keys,
+            query.astype(BF16),
+            kc[:, :, cols].reshape(places, DK),
             (((1,), (1,)), ((), ())),
             preferred_element_type=F32,
         )
-        mixing = (scores * decay_buf[head]).astype(BF16)
-        values = vc[:, :, cols].reshape(places, DK)
-        cached = jnp.dot(mixing, values, preferred_element_type=F32)
-        if j:
-            ca_send[j] = pack(cached)
-            ca_copies.append(to_kv(3, j, ca_send.at[j], ca_recv.at[j]))
-
+        mixing = (scores * decay_buf[h]).astype(BF16)
+        cached = jnp.dot(mixing, vc[:, :, cols].reshape(places, DK), preferred_element_type=F32)
+        ca_own[h] = cached
+        ca_send[h] = pack(cached)
+        for j in kv_order:
+            ca_copies[h, j] = to_kv(P_CA + h, j, ca_send.at[h], ca_recv.at[h, j])
+
+    loads["gg"].wait()
     for copy in kvg_copies:
         copy.wait_recv()
     own_head = pl.ds(pl.multiple_of(me_kv * DK, DK), DK)
     for j in kv_order:
         own_kvg = own_kvg + unpack(kvg_recv[j])
     own_kvg = own_kvg * factor
-    summed = [own_kvg[:, i * DK : (i + 1) * DK] for i in range(3)]
-    new_key, new_value, gate = summed
+    new_key, new_value, gate = [own_kvg[:, i * DK : (i + 1) * DK] for i in range(3)]
     front, back = rotate_in(new_key[:, :half], new_key[:, half:])
     query = q_full[:, own_head]
     score = jnp.sum(query[:, :half] * front + query[:, half:] * back, axis=1, keepdims=True)
-    own_term = score * new_value
-    gate = gate / (1.0 + jnp.exp(-gate))
-    totals = own_term + cached
-    for copy in ca_copies:
+    gate = gate / (1.0 + jnp.exp(-gate)) * gn_gain_ref[:, own_head]
+    ot_buf[me_kv, 0] = pack(score * new_value)
+    ot_buf[me_kv, 1] = pack(gate)
+    ot_copies = [to_kv(P_OT, j, ot_buf.at[me_kv], ot_buf.at[me_kv]) for j in kv_order]
+
+    loads["wo"].wait()
+    for copy in ot_copies:
         copy.wait_recv()
-    for j in range(1, n_kv):
-        totals = totals + unpack(ca_recv[j])
-    center = jnp.sum(totals, axis=1, keepdims=True) / DK
-    spread = jnp.sum(totals * totals, axis=1, keepdims=True) / DK - center * center
-    normed = (totals - center) * lax.rsqrt(spread + GN_EPS) * gn_gain_ref[:, own_head]
-    gt_buf[me_kv] = pack(gate * normed)
-    gt_copies = [to_kv(4, j, gt_buf.at[me_kv], gt_buf.at[me_kv]) for j in kv_order]
-
-    loads["wo"].wait()
-    for copy in gt_copies:
-        copy.wait_recv()
-    for c in range(n_kv):
-        x_buf[:, pl.ds(c * DK, DK)] = unpack(gt_buf[c]).astype(BF16)
-    o_buf[me_tp] = pack(jnp.dot(x_buf[...], wo[...], preferred_element_type=F32))
-    o_copies = [to_tp(1, j, o_buf.at[me_tp], o_buf.at[me_tp]) for j in tp_order]
-    for copy in o_copies:
-        copy.wait_recv()
+    out_part = None
+    for h in range(heads):
+        for j in kv_order:
+            ca_copies[h, j].wait_recv()
+        totals = ca_own[h] + unpack(ot_buf[h, 0])
+        for j in kv_order:
+            totals = totals + unpack(ca_recv[h, j])
+        center = jnp.sum(totals, axis=1, keepdims=True) / DK
+        spread = jnp.sum(totals * totals, axis=1, keepdims=True) / DK - center * center
+        normed = (totals - center) * lax.rsqrt(spread + GN_EPS)
+        x_buf[:, pl.ds(h * DK, DK)] = (unpack(ot_buf[h, 1]) * normed).astype(BF16)
+    out_part = jnp.dot(x_buf[...], wo[...], preferred_element_type=F32)
+    o_own[...] = out_part
+    o_send[...] = pack(out_part)
+    o_copy = to_tp(1, 1, o_send, o_recv)
+    o_copy.wait_recv()
+    chip_sum = o_own[...] + unpack(o_recv[...])
+    o_own[...] = chip_sum
+    chip_send[...] = pack(chip_sum)
+    chips = range(2, n_tp, 2)
+    relays = []
+    for j in chips:
+        for other in (1, 0):
+            relays.append(tp_copy(2, j + other, chip_send, chip_recv.at[j // 2], slot=j))
+
+    @pl.when(me_tp % 2 == 1)
+    def _():
+        for copy in relays:
+            copy.start()
+
+    loads["fg"].wait()
+    for j in chips:
+        relays[j - 2].wait_recv()
     squares = jnp.zeros((rows, 1), F32)
-    mixed = unpack(o_buf[0])
-    for t in range(1, n_tp):
-        mixed = mixed + unpack(o_buf[t])
+    mixed = o_own[...]
+    for j in chips:
+        mixed = mixed + unpack(chip_recv[j // 2])
     for c in range(n_tp):
         cols = pl.ds(c * own_cols, own_cols)
         own_mixed = mixed[:, c * own_cols : (c + 1) * own_cols]
@@ -443,22 +493,31 @@
         squares = squares + jnp.sum(resid_wide * resid_wide, axis=1, keepdims=True)
         x_buf[:, cols] = (resid_wide * ffn_gain_ref[:, cols]).astype(BF16)
     sqm_send[...] = jnp.broadcast_to(squares, (rows, LANES))
-    sqm_copies = [to_kv(5, j, sqm_send, sqm_recv.at[j]) for j in kv_order]
 
     x = x_buf[...]
     loads["wfg"].wait()
     loads["wfu"].wait()
-    gu_copies = []
-    for j in kv_order + (0,):
-        start = window_start(kv_peer(j), tiles, win // LANES, n_kv)
-        cols = pl.ds(pl.multiple_of(start * LANES, LANES), win)
-        both = []
+
+    def stage_start(s, index):
+        first, count = stages[s]
+        begin = first + window_start(index, count, STAGE_TILES, n_kv)
+        return pl.multiple_of(begin * LANES, LANES)
+
+    gu_copies = {}
+    sqm_copies = None
+    for s in range(len(stages)):
+        for j in kv_order:
+            cols = pl.ds(stage_start(s, kv_peer(j)), win)
+            for i, weight in enumerate((wfg, wfu)):
+                part = jnp.dot(x, weight[:, cols], preferred_element_type=F32)
+                gu_send[s, j, i] = pack(part)
+            gu_copies[s, j] = to_kv(P_GU + s, j, gu_send.at[s, j], gu_recv.at[s, j])
+        if sqm_copies is None:
+            sqm_copies = [to_kv(P_SQM, j, sqm_send, sqm_recv.at[j]) for j in kv_order]
+    for s in range(len(stages)):
+        cols = pl.ds(stage_start(s, me_kv), win)
         for i, weight in enumerate((wfg, wfu)):
-            part = jnp.dot(x, weight[:, cols], preferred_element_type=F32)
-            both.append(part)
-            if j:
-                gu_send[i, j] = pack(part)
-                gu_copies.append(to_kv(6 + 3 * i, j, gu_send.at[i, j], gu_recv.at[i, j]))
+            gu_own[s, i] = jnp.dot(x, weight[:, cols], preferred_element_type=F32)
 
     for copy in sqm_copies:
         copy.wait_recv()
@@ -466,38 +525,48 @@
     for j in range(1, n_kv):
         total_sq = total_sq + sqm_recv[j]
     factor = lax.rsqrt(total_sq / D + RMS_EPS)[:, :1]
-    for copy in gu_copies:
-        copy.wait_recv()
-    for i in range(2):
-        for j in kv_order:
-            both[i] = both[i] + unpack(gu_recv[i, j])
-    gate, up = both[0] * factor, both[1] * factor
-    hidden = gate / (1.0 + jnp.exp(-gate)) * up
-    here = window_start(me_kv, tiles, win // LANES, n_kv)
-    after = window_start(me_kv + 1, tiles, win // LANES, n_kv)
-    kept = jnp.where(me_kv == n_kv - 1, win, (after - here) * LANES)
-    column = lax.broadcasted_iota(jnp.int32, (rows, win), 1)
-    hid_buf[me_kv] = pack(jnp.where(column < kept, hidden, 0.0))
-    hid_copies = [to_kv(7, j, hid_buf.at[me_kv], hid_buf.at[me_kv]) for j in kv_order]
+    hid_copies = {}
+    for s in range(len(stages)):
+        for j in kv_order:
+            gu_copies[s, j].wait_recv()
+        both = []
+        for i in range(2):
+            total = gu_own[s, i]
+            for j in kv_order:
+                total = total + unpack(gu_recv[s, j, i])
+            both.append(total * factor)
+        gate, up = both
+        hidden = gate / (1.0 + jnp.exp(-gate)) * up
+        first, count = stages[s]
+        if count < STAGE_TILES * n_kv:
+            here, after = stage_start(s, me_kv), stage_start(s, me_kv + 1)
+            kept = jnp.where(me_kv == n_kv - 1, win, after - here)
+            column = lax.broadcasted_iota(jnp.int32, (rows, win), 1)
+            hidden = jnp.where(column < kept, hidden, 0.0)
+        hid_buf[s, 0] = pack(hidden)
+        for j in kv_order:
+            hid_copies[s, j] = to_kv(P_HID + s, j, hid_buf.at[s, 0], hid_buf.at[s, j])
 
     loads["wfd"].wait()
-    down = None
-    arrivals = dict(zip(kv_order, hid_copies))
-    for j in range(n_kv):
-        if j:
-            arrivals[j].wait_recv()
-        source = kv_peer(j)
-        start = window_start(source, tiles, win // LANES, n_kv)
-        weight = wfd[pl.ds(pl.multiple_of(start * LANES, LANES), win), :]
-        chunk = unpack(hid_buf[source]).astype(BF16)
-        part = jnp.dot(chunk, weight, preferred_element_type=F32)
-        down = part if down is None else down + part
+
+    def down_of(s, j):
+        weight = wfd[pl.ds(stage_start(s, kv_peer(j)), win), :]
+        chunk = unpack(hid_buf[s, j]).astype(BF16)
+        return jnp.dot(chunk, weight, preferred_element_type=F32)
+
+    down = down_of(0, 0)
+    for s in range(1, len(stages)):
+        down = down + down_of(s, 0)
+    for s in range(len(stages)):
+        for j in range(1, n_kv):
+            hid_copies[s, j].wait_recv()
+            down = down + down_of(s, j)
     down_buf[...] = down
     d_copies = {}
     for j in tp_order:
         cols = pl.ds(pl.multiple_of(tp_peer(j) * own_cols, own_cols), own_cols)
         d_send[j] = pack(down_buf[:, cols])
-        d_copies[j] = to_tp(2, j, d_send.at[j], d_recv.at[j])
+        d_copies[j] = to_tp(3, j, d_send.at[j], d_recv.at[j])
     own = pl.ds(pl.multiple_of(me_tp * own_cols, own_cols), own_cols)
     result = down_buf[:, own] + resid_buf[me_tp]
     for j in range(1, n_tp):
@@ -506,6 +575,11 @@
     out_ref[...] = result.astype(BF16)
     for copy in sent:
         copy.wait_send()
+
+    @pl.when(me_tp % 2 == 1)
+    def _():
+        for copy in relays:
+            copy.wait_send()
 
 
 def fused(
@@ -530,13 +604,20 @@
 ):
     rows, own_cols = tokens.shape
     depth, wide = w_query.shape
-    units = w_ffn_gate.shape[1]
-    tiles = units // LANES
-    win = -(-tiles // n_kv // 2) * 2 * LANES
     span = key_cache.shape[1]
+    heads = log_decay.shape[0]
+    win = STAGE_TILES * LANES
+    n_stage = len(stage_spans(w_ffn_gate.shape[1] // LANES, n_kv))
     vmem = pl.BlockSpec(memory_space=pltpu.VMEM)
-    smem = pl.BlockSpec(memory_space=pltpu.SMEM)
     hbm = pl.BlockSpec(memory_space=pl.ANY)
+    small = (
+        tokens,
+        lengths,
+        attn_gain[None, :],
+        log_decay,
+        gn_gain[None, :],
+        ffn_gain[None, :],
+    )
     streamed = (
         w_query,
         w_key,
@@ -549,63 +630,66 @@
         w_ffn_up,
         w_ffn_down,
     )
+    kv_phases = 4 + 2 * heads + 2 * n_stage
     scratch = [pltpu.VMEM(a.shape, a.dtype) for a in streamed] + [
+        (pltpu.SMEM if a.ndim == 1 else pltpu.VMEM)(a.shape, a.dtype) for a in small
+    ]
+    scratch += [
         pltpu.VMEM((n_tp, rows, own_cols), BF16),
         pltpu.VMEM((rows, depth), BF16),
         pltpu.VMEM((rows, LANES), F32),
         pltpu.VMEM((n_kv, rows, LANES), F32),
-        pltpu.VMEM((2, 2 * rows, wide // 4), BF16),
-        pltpu.VMEM((2, n_kv, 2 * rows, wide // 4), BF16),
+        pltpu.VMEM((heads, 2 * rows, DK // 2), BF16),
+        pltpu.VMEM((heads, n_kv, 2 * rows, DK // 2), BF16),
         pltpu.VMEM((rows, wide), F32),
         pltpu.VMEM((2, rows, DK // 2), F32),
-        pltpu.VMEM((n_kv, rows, rows * span), F32),
+        pltpu.VMEM((heads, rows, rows * span), F32),
         pltpu.VMEM((n_kv, 2 * rows, 3 * DK // 2), BF16),
         pltpu.VMEM((n_kv, 2 * rows, 3 * DK // 2), BF16),
-        pltpu.VMEM((n_kv, 2 * rows, DK // 2), BF16),
-        pltpu.VMEM((n_kv, 2 * rows, DK // 2), BF16),
-        pltpu.VMEM((n_kv, 2 * rows, DK // 2), BF16),
-        pltpu.VMEM((n_tp, 2 * rows, depth // 2), BF16),
+        pltpu.VMEM((heads, rows, DK), F32),
+        pltpu.VMEM((heads, 2 * rows, DK // 2), BF16),
+        pltpu.VMEM((heads, n_kv, 2 * rows, DK // 2), BF16),
+        pltpu.VMEM((n_kv, 2, 2 * rows, DK // 2), BF16),
+        pltpu.VMEM((rows, depth), F32),
+        pltpu.VMEM((2 * rows, depth // 2), BF16),
+        pltpu.VMEM((2 * rows, depth // 2), BF16),
+        pltpu.VMEM((2 * rows, depth // 2), BF16),
+        pltpu.VMEM((n_tp // 2, 2 * rows, depth // 2), BF16),
         pltpu.VMEM((n_tp, rows, own_cols), F32),
         pltpu.VMEM((rows, LANES), F32),
         pltpu.VMEM((n_kv, rows, LANES), F32),
-        pltpu.VMEM((2, n_kv, 2 * rows, win // 2), BF16),
-        pltpu.VMEM((2, n_kv, 2 * rows, win // 2), BF16),
-        pltpu.VMEM((n_kv, 2 * rows, win // 2), BF16),
+        pltpu.VMEM((n_stage, 2, rows, win), F32),
+        pltpu.VMEM((n_stage, n_kv, 2, 2 * rows, win // 2), BF16),
+        pltpu.VMEM((n_stage, n_kv, 2, 2 * rows, win // 2), BF16),
+        pltpu.VMEM((n_stage, n_kv, 2 * rows, win // 2), BF16),
         pltpu.VMEM((rows, depth), F32),
         pltpu.VMEM((n_tp, 2 * rows, own_cols // 2), BF16),
         pltpu.VMEM((n_tp, 2 * rows, own_cols // 2), BF16),
-        pltpu.SemaphoreType.DMA((len(streamed),)),
-        pltpu.SemaphoreType.DMA((10, n_kv)),
-        pltpu.SemaphoreType.DMA((10, n_kv)),
-        pltpu.SemaphoreType.DMA((3, n_tp)),
-        pltpu.SemaphoreType.DMA((3, n_tp)),
+        pltpu.SemaphoreType.DMA((len(small) + len(streamed),)),
+        pltpu.SemaphoreType.DMA((kv_phases, n_kv)),
+        pltpu.SemaphoreType.DMA((kv_phases, n_kv)),
+        pltpu.SemaphoreType.DMA((4, n_tp)),
+        pltpu.SemaphoreType.DMA((4, n_tp)),
     ]
     return pl.pallas_call(
         functools.partial(layer_kernel, n_kv, n_tp),
         out_shape=pltpu.VMEM((rows, own_cols), BF16),
-        in_specs=[vmem, smem, vmem, smem, vmem, vmem] + [hbm] * len(streamed),
+        in_specs=[hbm] * (len(small) + len(streamed)),
         out_specs=vmem,
         scratch_shapes=scratch,
         compiler_params=pltpu.CompilerParams(
             collective_id=0, has_side_effects=True, vmem_limit_bytes=60 * 1024 * 1024
         ),
-    )(
-        tokens,
-        lengths,
-        attn_gain[None, :],
-        log_decay,
-        gn_gain[None, :],
-        ffn_gain[None, :],
-        *streamed,
-    )
+    )(*small, *streamed)
 
 
 def fits(mesh, tokens, log_decay, key_cache, w_query, w_ffn_gate):
     n_kv, n_tp, n_grp = mesh.shape["kv"], mesh.shape["tp"], mesh.shape["grp"]
     heads, span = log_decay.shape[0], key_cache.shape[1] // n_kv
+    tiles = w_ffn_gate.shape[1] // n_tp // LANES
     return (
         n_kv > 1
-        and n_tp > 1
+        and n_tp > 2
         and n_kv & (n_kv - 1) == 0
         and n_tp & (n_tp - 1) == 0
         and heads == n_kv * n_tp
@@ -613,6 +697,7 @@
         and tokens.shape[1] % (n_kv * n_tp * 2 * LANES) == 0
         and heads * DK // n_tp % (4 * LANES) == 0
         and w_ffn_gate.shape[1] % (n_tp * LANES) == 0
+        and stage_spans(tiles, n_kv)[-1][1] >= STAGE_TILES
         and tokens.shape[0] // n_grp % 8 == 0
         and span % 16 == 0
         and span <= 64

time: 48.8 us -> 49.9 us (1.023)
  Pallas kernels: 48 us -> 49.1 us
    pallas_call x1, Pallas kernels: 48 us -> 49.1 us  [fused(): pl.pallas_call(functools.partial(layer_kernel, n_kv, n_tp), out_shape=plt...]
where the time goes in v1:
time: 49.9 us; the launch traced here: 49.7 us
  Pallas kernels  49.1 us (98%)
  local copies, waits for them, and re-layouts  0.6 us (1%)
    pallas_call x1, Pallas kernels, fused(): pl.pallas_call(functools.partial(layer_kernel, n_kv, n_tp), out_shape=plt...  49.1 us

profile of v1, /device:TPU:0, one launch (start us, length us, event | category | flops | bytes accessed | tf_op | source)
XLA Modules:
  0.0 49.7 jit_solution(3438130553693914865)
XLA Ops:
  0.0 49.1 %shard_map.154 = bf16[24,256]{1,0:T(8,128)(2,1)S(1)} custom-call(bf16[24,256]{1,0:T(8,128)(2,1)} %tokens_hbm.1, s32[24]{0:T(128)} %lengths_hbm.1, f32[1,1024]{1,0:T(1,128)} %bitcast.3, f32[4]{0:T(128)} %log_decay_hbm.1, f32[1,1024]{1,0:T(1,128)} %bitcast.4, f32[1,1024]{1,0:T(1,128)} %bitcast.5, bf16[1024,1024]{1,0:T(8,128)(2,1)} %wq_hbm.1, ...), custom_call_target="tpu_custom_call" | custom-call | tf_op jit(solution)/shard_map/pallas_call | solution.py:674
  49.1 0.6 %copy.18 = bf16[24,256]{1,0:T(8,128)(2,1)} copy(bf16[24,256]{1,0:T(8,128)(2,1)S(1)} %shard_map.154) | data formatting | bytes 24576

commit v2 on v1

--- a/solution.py
+++ b/solution.py
@@ -204,17 +204,16 @@
     q_full,
     trig,
     decay_buf,
-    kvg_send,
-    kvg_recv,
-    ca_own,
+    key_own,
+    vg_send,
+    vg_in,
     ca_send,
-    ca_recv,
-    ot_buf,
-    o_own,
-    o_send,
-    o_recv,
-    chip_send,
-    chip_recv,
+    ca_in,
+    sc_send,
+    sc_in,
+    gt_send,
+    gt_buf,
+    o_buf,
     resid_buf,
     sqm_send,
     sqm_recv,
@@ -230,6 +229,10 @@
     kv_recv_sem,
     tp_send_sem,
     tp_recv_sem,
+    own_send_sem,
+    own_recv_sem,
+    gt_send_sem,
+    gt_recv_sem,
 ):
     rows, own_cols = tokens_ref.shape
     depth, wide = wq.shape
@@ -239,8 +242,13 @@
     win = STAGE_TILES * LANES
     stages = stage_spans(tiles, n_kv)
     heads = n_kv
+    middle = n_kv // 2 - 1
+    shared = heads // 2
     me_kv = lax.axis_index("kv")
     me_tp = lax.axis_index("tp")
+    me_core = me_tp % 2
+    first_core = me_tp - me_core
+    is_owner = (me_core == 1) & (me_kv >= middle) & (me_kv < middle + 2)
 
     def kv_peer(j):
         return partner(me_kv, j, n_kv)
@@ -255,6 +263,12 @@
     for j in range(1, n_kv):
         pl.semaphore_signal(
             barrier, inc=1, device_id={"kv": kv_peer(j)}, device_id_type=pl.DeviceIdType.MESH
+        )
+        pl.semaphore_signal(
+            barrier,
+            inc=1,
+            device_id={"kv": kv_peer(j), "tp": tp_peer(1)},
+            device_id_type=pl.DeviceIdType.MESH,
         )
     for j in range(1, n_tp):
         pl.semaphore_signal(
@@ -299,31 +313,91 @@
         sent.append(copy)
         return copy
 
-    def tp_copy(phase, j, src, dst, slot=None):
+    def tp_waiter(phase, j, ref):
+        return pltpu.make_async_remote_copy(
+            src_ref=ref,
+            dst_ref=ref,
+            send_sem=tp_send_sem.at[phase, j],
+            recv_sem=tp_recv_sem.at[phase, tp_peer(j)],
+            device_id={"tp": tp_peer(j)},
+            device_id_type=pl.DeviceIdType.MESH,
+        )
+
+    def tp_target(place):
+        chip, core = place
+        return partner(first_core, 2 * chip, n_tp) + core
+
+    far = [(chip, core) for chip in range(n_tp // 2 - 1, 0, -1) for core in (0, 1)]
+
+    def to_tp(phase, src_of, dst):
+        def send(target, slot):
+            copy = pltpu.make_async_remote_copy(
+                src_ref=src_of(target),
+                dst_ref=dst,
+                send_sem=tp_send_sem.at[phase, slot],
+                recv_sem=tp_recv_sem.at[phase, me_tp],
+                device_id={"tp": target},
+                device_id_type=pl.DeviceIdType.MESH,
+            )
+            copy.start()
+            sent.append(copy)
+
+        for slot, place in enumerate(far):
+            send(tp_target(place), slot)
+        send(tp_peer(1), len(far))
+
+    def owner_copy(kind, h, src, dst):
+        slot = own_send_sem.at[kind, h]
         return pltpu.make_async_remote_copy(
             src_ref=src,
             dst_ref=dst,
-            send_sem=tp_send_sem.at[phase, j],
-            recv_sem=tp_recv_sem.at[phase, j if slot is None else slot],
-            device_id={"tp": tp_peer(j)},
+            send_sem=slot,
+            recv_sem=own_recv_sem.at[kind, me_core, me_kv, h % shared],
+            device_id={"kv": middle + h // shared, "tp": first_core + 1},
             device_id_type=pl.DeviceIdType.MESH,
         )
 
-    def to_tp(phase, j, src, dst):
-        copy = tp_copy(phase, j, src, dst)
-        copy.start()
-        sent.append(copy)
-        return copy
-
-    P_SQ, P_Q, P_KVG, P_CA, P_OT = 0, 1, 1 + heads, 2 + heads, 2 + 2 * heads
-    P_SQM, P_GU, P_HID = 3 + 2 * heads, 4 + 2 * heads, 4 + 2 * heads + len(stages)
+    def owns(h):
+        return (me_core == 1) & (me_kv == middle + h // shared)
+
+    def to_owner(pairs):
+        for h, copies in pairs:
+
+            @pl.when(jnp.logical_not(owns(h)))
+            def _():
+                for copy in copies:
+                    copy.start()
+
+            to_owners.append((h, copies))
+
+    to_owners = []
+    VG, CA, SC = 0, 1, 2
+
+    def column_tile(columns):
+        lane_id = lax.broadcasted_iota(jnp.int32, (8, LANES), 1)
+        tile = jnp.zeros((8, LANES), F32)
+        groups = rows // 8
+        for i, column in enumerate(columns):
+            for r in range(groups):
+                part = jnp.broadcast_to(column[r * 8 : (r + 1) * 8], (8, LANES))
+                tile = jnp.where(lane_id == i * groups + r, part, tile)
+        return tile
+
+    def tile_column(tile, i):
+        groups = rows // 8
+        return jnp.concatenate(
+            [tile[:, i * groups + r : i * groups + r + 1] for r in range(groups)], axis=0
+        )
+
+    P_SQ, P_Q = 0, 1
+    P_SQM, P_GU, P_HID = 1 + heads, 2 + heads, 2 + heads + len(stages)
 
     for name in ("tok", "len", "ld", "ag", "wq"):
         loads[name].start()
     loads["tok"].wait()
-    pl.semaphore_wait(barrier, n_kv + n_tp - 2)
-
-    tok_copies = [to_tp(0, j, tokens_ref, tok_buf.at[me_tp]) for j in tp_order]
+    pl.semaphore_wait(barrier, 2 * (n_kv - 1) + n_tp - 1)
+
+    to_tp(0, lambda target: tokens_ref, tok_buf.at[me_tp])
     for name in ("wk", "wv", "wg", "kc", "vc", "gg", "fg"):
         loads[name].start()
     tok_buf[me_tp] = tokens_ref[...]
@@ -354,56 +428,51 @@
         cosine, sine = trig[0], trig[1]
         return front * cosine - back * sine, front * sine + back * cosine
 
-    for copy in tok_copies:
-        copy.wait_recv()
+    for j in tp_order:
+        tp_waiter(0, j, tokens_ref).wait_recv()
     squares = jnp.zeros((rows, 1), F32)
     for c in range(n_tp):
         wide_tok = tok_buf[c].astype(F32)
         squares = squares + jnp.sum(wide_tok * wide_tok, axis=1, keepdims=True)
         cols = pl.ds(c * own_cols, own_cols)
         x_buf[:, cols] = (wide_tok * attn_gain_ref[:, cols]).astype(BF16)
-    sq_send[...] = jnp.broadcast_to(squares, (rows, LANES))
+    sq_send[...] = column_tile([squares])
+    sq_copies = [to_kv(P_SQ, j, sq_send, sq_recv.at[j]) for j in kv_order]
 
     x = x_buf[...]
     loads["wq"].wait()
     q_copies = {}
-    sq_copies = None
-    for h in range(heads):
-        cols = pl.ds(h * DK, DK)
-        q_own = jnp.dot(x, wq[:, cols], preferred_element_type=F32)
-        q_send[h] = pack(q_own)
-        q_full[:, cols] = q_own
-        for j in kv_order:
-            q_copies[h, j] = to_kv(P_Q + h, j, q_send.at[h], q_recv.at[h, j])
-        if sq_copies is None:
-            sq_copies = [to_kv(P_SQ, j, sq_send, sq_recv.at[j]) for j in kv_order]
+    for pair in range(heads // 2):
+        q_own = jnp.dot(x, wq[:, pl.ds(pair * 2 * DK, 2 * DK)], preferred_element_type=F32)
+        for i in range(2):
+            h = pair * 2 + i
+            piece = q_own[:, i * DK : (i + 1) * DK]
+            q_send[h] = pack(piece)
+            q_full[:, pl.ds(h * DK, DK)] = piece
+            for j in kv_order:
+                q_copies[h, j] = to_kv(P_Q + h, j, q_send.at[h], q_recv.at[h, j])
     for name in ("wo", "wfg", "wfu", "wfd"):
         loads[name].start()
 
     for name in ("wk", "wv", "wg"):
         loads[name].wait()
-    kvg_copies = []
-    for j in kv_order + (0,):
-        cols = pl.ds(pl.multiple_of(kv_peer(j) * DK, DK), DK)
-        parts = [
-            jnp.dot(x, weight[:, cols], preferred_element_type=F32) for weight in (wk, wv, wg)
-        ]
-        if j:
-            kvg_send[j] = pack(jnp.concatenate(parts, axis=1))
-            kvg_copies.append(to_kv(P_KVG, j, kvg_send.at[j], kvg_recv.at[j]))
-        else:
-            own_kvg = jnp.concatenate(parts, axis=1)
+    for i, weight in enumerate((wv, wg)):
+        for pair in range(heads // 2):
+            part = jnp.dot(x, weight[:, pl.ds(pair * 2 * DK, 2 * DK)], preferred_element_type=F32)
+            for k in range(2):
+                vg_send[pair * 2 + k, i] = pack(part[:, k * DK : (k + 1) * DK])
+    key_own[...] = jnp.dot(x, wk[...], preferred_element_type=F32)
 
     for copy in sq_copies:
         copy.wait_recv()
     total_sq = sq_send[...]
     for j in range(1, n_kv):
         total_sq = total_sq + sq_recv[j]
-    factor = lax.rsqrt(total_sq / D + RMS_EPS)[:, :1]
+    factor = lax.rsqrt(tile_column(total_sq, 0) / D + RMS_EPS)
 
     loads["kc"].wait()
     loads["vc"].wait()
-    ca_copies = {}
+    own_scores = []
     for h in range(heads):
         cols = pl.ds(h * DK, DK)
         for j in kv_order:
@@ -414,7 +483,6 @@
         query = query * factor
         front, back = rotate_in(query[:, :half], query[:, half:])
         query = jnp.concatenate([front, back], axis=1) * DK ** (-0.5)
-        q_full[:, cols] = query
         scores = lax.dot_general(
             query.astype(BF16),
             kc[:, :, cols].reshape(places, DK),
@@ -423,67 +491,142 @@
         )
         mixing = (scores * decay_buf[h]).astype(BF16)
         cached = jnp.dot(mixing, vc[:, :, cols].reshape(places, DK), preferred_element_type=F32)
-        ca_own[h] = cached
         ca_send[h] = pack(cached)
-        for j in kv_order:
-            ca_copies[h, j] = to_kv(P_CA + h, j, ca_send.at[h], ca_recv.at[h, j])
-
+        key = key_own[:, cols]
+        front, back = rotate_in(key[:, :half], key[:, half:])
+        own_scores.append(
+            jnp.sum(query[:, :half] * front + query[:, half:] * back, axis=1, keepdims=True)
+            * factor
+        )
+        pairs = [(h, [owner_copy(CA, h, ca_send.at[h], ca_in.at[me_core, me_kv, h % shared])])]
+        if h % shared == shared - 1:
+            oi = h // shared
+            sc_send[oi] = column_tile(own_scores[oi * shared :])
+            pairs[0][1].append(owner_copy(SC, oi * shared, sc_send.at[oi], sc_in.at[me_core, me_kv]))
+        to_owner(pairs)
+        if h == 0:
+            to_owner(
+                [
+                    (
+                        g,
+                        [
+                            owner_copy(
+                                VG, g, vg_send.at[g], vg_in.at[me_core, me_kv, g % shared]
+                            )
+                        ],
+                    )
+                    for g in range(heads)
+                ]
+            )
+
+    def owned(c, kind, hh, j, ref):
+        at = me_kv if j == 0 else kv_peer(j)
+        return pltpu.make_async_remote_copy(
+            src_ref=ref,
+            dst_ref=ref,
+            send_sem=own_send_sem.at[kind, 0],
+            recv_sem=own_recv_sem.at[kind, c, at, hh],
+            device_id={"kv": kv_peer(1)},
+            device_id_type=pl.DeviceIdType.MESH,
+        )
+
+    def gt_copies(c, hh, head):
+        peers = kv_order + ((0,) if c == 0 else ())
+        return [
+            pltpu.make_async_remote_copy(
+                src_ref=gt_send.at[c, hh],
+                dst_ref=gt_buf.at[head],
+                send_sem=gt_send_sem.at[c, hh, j],
+                recv_sem=gt_recv_sem.at[head],
+                device_id={"kv": me_kv if j == 0 else kv_peer(j), "tp": first_core + c},
+                device_id_type=pl.DeviceIdType.MESH,
+            )
+            for j in peers
+        ]
+
+    @pl.when(is_owner)
+    def _():
+        base = (me_kv - middle) * shared
+        units = [(c, hh) for c in (1, 0) for hh in range(shared)]
+        for c, hh in units:
+            for j in kv_order + ((0,) if c == 0 else ()):
+                owned(c, VG, hh, j, vg_in.at[0, 0, 0]).wait_recv()
+        gates, news = {}, {}
+        for c, hh in units:
+            if c:
+                both = [unpack(vg_send[base + hh, i]) for i in range(2)]
+            else:
+                both = [unpack(vg_in[0, me_kv, hh, i]) for i in range(2)]
+            for j in kv_order:
+                both = [both[i] + unpack(vg_in[c, kv_peer(j), hh, i]) for i in range(2)]
+            new_value, gate = both[0] * factor, both[1] * factor
+            news[c, hh] = new_value
+            gates[c, hh] = gate / (1.0 + jnp.exp(-gate))
+        for c in (1, 0):
+            for j in kv_order + ((0,) if c == 0 else ()):
+                owned(c, SC, 0, j, sc_in.at[0, 0]).wait_recv()
+        for c, hh in units:
+            for j in kv_order + ((0,) if c == 0 else ()):
+                owned(c, CA, hh, j, ca_in.at[0, 0, 0]).wait_recv()
+            if c:
+                totals = unpack(ca_send[base + hh])
+                tile = sc_send[me_kv - middle]
+            else:
+                totals = unpack(ca_in[0, me_kv, hh])
+                tile = sc_in[0, me_kv]
+            for j in kv_order:
+                totals = totals + unpack(ca_in[c, kv_peer(j), hh])
+                tile = tile + sc_in[c, kv_peer(j)]
+            totals = totals + tile_column(tile, hh) * news[c, hh]
+            center = jnp.sum(totals, axis=1, keepdims=True) / DK
+            spread = jnp.sum(totals * totals, axis=1, keepdims=True) / DK - center * center
+            normed = (totals - center) * lax.rsqrt(spread + GN_EPS)
+            result = pack(gates[c, hh] * normed)
+            gt_send[c, hh] = result
+            if c:
+                gt_buf[base + hh] = result
+            for copy in gt_copies(c, hh, base + hh):
+                copy.start()
+
+    loads["wo"].wait()
     loads["gg"].wait()
-    for copy in kvg_copies:
-        copy.wait_recv()
-    own_head = pl.ds(pl.multiple_of(me_kv * DK, DK), DK)
-    for j in kv_order:
-        own_kvg = own_kvg + unpack(kvg_recv[j])
-    own_kvg = own_kvg * factor
-    new_key, new_value, gate = [own_kvg[:, i * DK : (i + 1) * DK] for i in range(3)]
-    front, back = rotate_in(new_key[:, :half], new_key[:, half:])
-    query = q_full[:, own_head]
-    score = jnp.sum(query[:, :half] * front + query[:, half:] * back, axis=1, keepdims=True)
-    gate = gate / (1.0 + jnp.exp(-gate)) * gn_gain_ref[:, own_head]
-    ot_buf[me_kv, 0] = pack(score * new_value)
-    ot_buf[me_kv, 1] = pack(gate)
-    ot_copies = [to_kv(P_OT, j, ot_buf.at[me_kv], ot_buf.at[me_kv]) for j in kv_order]
-
-    loads["wo"].wait()
-    for copy in ot_copies:
-        copy.wait_recv()
-    out_part = None
     for h in range(heads):
-        for j in kv_order:
-            ca_copies[h, j].wait_recv()
-        totals = ca_own[h] + unpack(ot_buf[h, 0])
-        for j in kv_order:
-            totals = totals + unpack(ca_recv[h, j])
-        center = jnp.sum(totals, axis=1, keepdims=True) / DK
-        spread = jnp.sum(totals * totals, axis=1, keepdims=True) / DK - center * center
-        normed = (totals - center) * lax.rsqrt(spread + GN_EPS)
-        x_buf[:, pl.ds(h * DK, DK)] = (unpack(ot_buf[h, 1]) * normed).astype(BF16)
-    out_part = jnp.dot(x_buf[...], wo[...], preferred_element_type=F32)
-    o_own[...] = out_part
-    o_send[...] = pack(out_part)
-    o_copy = to_tp(1, 1, o_send, o_recv)
-    o_copy.wait_recv()
-    chip_sum = o_own[...] + unpack(o_recv[...])
-    o_own[...] = chip_sum
-    chip_send[...] = pack(chip_sum)
-    chips = range(2, n_tp, 2)
-    relays = []
-    for j in chips:
-        for other in (1, 0):
-            relays.append(tp_copy(2, j + other, chip_send, chip_recv.at[j // 2], slot=j))
-
-    @pl.when(me_tp % 2 == 1)
-    def _():
-        for copy in relays:
-            copy.start()
-
+        waiter = pltpu.make_async_remote_copy(
+            src_ref=gt_send.at[0, 0],
+            dst_ref=gt_buf.at[h],
+            send_sem=gt_send_sem.at[0, 0, 0],
+            recv_sem=gt_recv_sem.at[h],
+            device_id={"kv": kv_peer(1)},
+            device_id_type=pl.DeviceIdType.MESH,
+        )
+
+        @pl.when(jnp.logical_not(owns(h)))
+        def _():
+            waiter.wait_recv()
+
+    for h in range(heads):
+        cols = pl.ds(h * DK, DK)
+        x_buf[:, cols] = (unpack(gt_buf[h]) * gn_gain_ref[:, cols]).astype(BF16)
+    gated = x_buf[...]
+    for part in range(2):
+        width = depth // 2
+        piece = jnp.dot(
+            gated, wo[:, pl.ds(part * width, width)], preferred_element_type=F32
+        )
+        o_buf[part, me_tp] = pack(piece)
+        to_tp(1 + part, lambda target: o_buf.at[part, me_tp], o_buf.at[part, me_tp])
     loads["fg"].wait()
-    for j in chips:
-        relays[j - 2].wait_recv()
+    for part in range(2):
+        for j in tp_order:
+            tp_waiter(1 + part, j, o_buf.at[part, 0]).wait_recv()
     squares = jnp.zeros((rows, 1), F32)
-    mixed = o_own[...]
-    for j in chips:
-        mixed = mixed + unpack(chip_recv[j // 2])
+    halves = []
+    for part in range(2):
+        total = unpack(o_buf[part, 0])
+        for t in range(1, n_tp):
+            total = total + unpack(o_buf[part, t])
+        halves.append(total)
+    mixed = jnp.concatenate(halves, axis=1)
     for c in range(n_tp):
         cols = pl.ds(c * own_cols, own_cols)
         own_mixed = mixed[:, c * own_cols : (c + 1) * own_cols]
@@ -492,7 +635,8 @@
         resid_buf[c] = resid_wide
         squares = squares + jnp.sum(resid_wide * resid_wide, axis=1, keepdims=True)
         x_buf[:, cols] = (resid_wide * ffn_gain_ref[:, cols]).astype(BF16)
-    sqm_send[...] = jnp.broadcast_to(squares, (rows, LANES))
+    sqm_send[...] = column_tile([squares])
+    sqm_copies = [to_kv(P_SQM, j, sqm_send, sqm_recv.at[j]) for j in kv_order]
 
     x = x_buf[...]
     loads["wfg"].wait()
@@ -504,7 +648,6 @@
         return pl.multiple_of(begin * LANES, LANES)
 
     gu_copies = {}
-    sqm_copies = None
     for s in range(len(stages)):
         for j in kv_order:
             cols = pl.ds(stage_start(s, kv_peer(j)), win)
@@ -512,8 +655,6 @@
                 part = jnp.dot(x, weight[:, cols], preferred_element_type=F32)
                 gu_send[s, j, i] = pack(part)
             gu_copies[s, j] = to_kv(P_GU + s, j, gu_send.at[s, j], gu_recv.at[s, j])
-        if sqm_copies is None:
-            sqm_copies = [to_kv(P_SQM, j, sqm_send, sqm_recv.at[j]) for j in kv_order]
     for s in range(len(stages)):
         cols = pl.ds(stage_start(s, me_kv), win)
         for i, weight in enumerate((wfg, wfu)):
@@ -524,7 +665,7 @@
     total_sq = sqm_send[...]
     for j in range(1, n_kv):
         total_sq = total_sq + sqm_recv[j]
-    factor = lax.rsqrt(total_sq / D + RMS_EPS)[:, :1]
+    factor = lax.rsqrt(tile_column(total_sq, 0) / D + RMS_EPS)
     hid_copies = {}
     for s in range(len(stages)):
         for j in kv_order:
@@ -562,24 +703,32 @@
             hid_copies[s, j].wait_recv()
             down = down + down_of(s, j)
     down_buf[...] = down
-    d_copies = {}
-    for j in tp_order:
-        cols = pl.ds(pl.multiple_of(tp_peer(j) * own_cols, own_cols), own_cols)
-        d_send[j] = pack(down_buf[:, cols])
-        d_copies[j] = to_tp(3, j, d_send.at[j], d_recv.at[j])
+    for t in range(n_tp):
+        d_send[t] = pack(down_buf[:, pl.ds(t * own_cols, own_cols)])
+    to_tp(3, lambda target: d_send.at[target], d_recv.at[me_tp])
     own = pl.ds(pl.multiple_of(me_tp * own_cols, own_cols), own_cols)
     result = down_buf[:, own] + resid_buf[me_tp]
     for j in range(1, n_tp):
-        d_copies[j].wait_recv()
-        result = result + unpack(d_recv[j])
+        tp_waiter(3, j, d_recv.at[0]).wait_recv()
+        result = result + unpack(d_recv[tp_peer(j)])
     out_ref[...] = result.astype(BF16)
     for copy in sent:
         copy.wait_send()
-
-    @pl.when(me_tp % 2 == 1)
+    for h in range(heads):
+
+        @pl.when(jnp.logical_not(owns(h)))
+        def _():
+            for head, copies in to_owners:
+                if head == h:
+                    for copy in copies:
+                        copy.wait_send()
+
+    @pl.when(is_owner)
     def _():
-        for copy in relays:
-            copy.wait_send()
+        for c in (1, 0):
+            for hh in range(shared):
+                for copy in gt_copies(c, hh, hh):
+                    copy.wait_send()
 
 
 def fused(
@@ -606,6 +755,7 @@
     depth, wide = w_query.shape
     span = key_cache.shape[1]
     heads = log_decay.shape[0]
+    shared = heads // 2
     win = STAGE_TILES * LANES
     n_stage = len(stage_spans(w_ffn_gate.shape[1] // LANES, n_kv))
     vmem = pl.BlockSpec(memory_space=pltpu.VMEM)
@@ -630,34 +780,33 @@
         w_ffn_up,
         w_ffn_down,
     )
-    kv_phases = 4 + 2 * heads + 2 * n_stage
+    kv_phases = 2 + heads + 2 * n_stage
     scratch = [pltpu.VMEM(a.shape, a.dtype) for a in streamed] + [
         (pltpu.SMEM if a.ndim == 1 else pltpu.VMEM)(a.shape, a.dtype) for a in small
     ]
     scratch += [
         pltpu.VMEM((n_tp, rows, own_cols), BF16),
         pltpu.VMEM((rows, depth), BF16),
-        pltpu.VMEM((rows, LANES), F32),
-        pltpu.VMEM((n_kv, rows, LANES), F32),
+        pltpu.VMEM((8, LANES), F32),
+        pltpu.VMEM((n_kv, 8, LANES), F32),
         pltpu.VMEM((heads, 2 * rows, DK // 2), BF16),
         pltpu.VMEM((heads, n_kv, 2 * rows, DK // 2), BF16),
         pltpu.VMEM((rows, wide), F32),
         pltpu.VMEM((2, rows, DK // 2), F32),
         pltpu.VMEM((heads, rows, rows * span), F32),
-        pltpu.VMEM((n_kv, 2 * rows, 3 * DK // 2), BF16),
-        pltpu.VMEM((n_kv, 2 * rows, 3 * DK // 2), BF16),
-        pltpu.VMEM((heads, rows, DK), F32),
+        pltpu.VMEM((rows, wide), F32),
+        pltpu.VMEM((heads, 2, 2 * rows, DK // 2), BF16),
+        pltpu.VMEM((2, n_kv, shared, 2, 2 * rows, DK // 2), BF16),
         pltpu.VMEM((heads, 2 * rows, DK // 2), BF16),
-        pltpu.VMEM((heads, n_kv, 2 * rows, DK // 2), BF16),
-        pltpu.VMEM((n_kv, 2, 2 * rows, DK // 2), BF16),
-        pltpu.VMEM((rows, depth), F32),
-        pltpu.VMEM((2 * rows, depth // 2), BF16),
-        pltpu.VMEM((2 * rows, depth // 2), BF16),
-        pltpu.VMEM((2 * rows, depth // 2), BF16),
-        pltpu.VMEM((n_tp // 2, 2 * rows, depth // 2), BF16),
+        pltpu.VMEM((2, n_kv, shared, 2 * rows, DK // 2), BF16),
+        pltpu.VMEM((2, 8, LANES), F32),
+        pltpu.VMEM((2, n_kv, 8, LANES), F32),
+        pltpu.VMEM((2, shared, 2 * rows, DK // 2), BF16),
+        pltpu.VMEM((heads, 2 * rows, DK // 2), BF16),
+        pltpu.VMEM((2, n_tp, 2 * rows, depth // 4), BF16),
         pltpu.VMEM((n_tp, rows, own_cols), F32),
-        pltpu.VMEM((rows, LANES), F32),
-        pltpu.VMEM((n_kv, rows, LANES), F32),
+        pltpu.VMEM((8, LANES), F32),
+        pltpu.VMEM((n_kv, 8, LANES), F32),
         pltpu.VMEM((n_stage, 2, rows, win), F32),
         pltpu.VMEM((n_stage, n_kv, 2, 2 * rows, win // 2), BF16),
         pltpu.VMEM((n_stage, n_kv, 2, 2 * rows, win // 2), BF16),
@@ -670,6 +819,10 @@
         pltpu.SemaphoreType.DMA((kv_phases, n_kv)),
         pltpu.SemaphoreType.DMA((4, n_tp)),
         pltpu.SemaphoreType.DMA((4, n_tp)),
+        pltpu.SemaphoreType.DMA((3, heads)),
+        pltpu.SemaphoreType.DMA((3, 2, n_kv, shared)),
+        pltpu.SemaphoreType.DMA((2, shared, n_kv)),
+        pltpu.SemaphoreType.DMA((heads,)),
     ]
     return pl.pallas_call(
         functools.partial(layer_kernel, n_kv, n_tp),
@@ -687,12 +840,14 @@
     n_kv, n_tp, n_grp = mesh.shape["kv"], mesh.shape["tp"], mesh.shape["grp"]
     heads, span = log_decay.shape[0], key_cache.shape[1] // n_kv
     tiles = w_ffn_gate.shape[1] // n_tp // LANES
+    rows = tokens.shape[0] // n_grp
     return (
         n_kv > 1
         and n_tp > 2
         and n_kv & (n_kv - 1) == 0
         and n_tp & (n_tp - 1) == 0
         and heads == n_kv * n_tp
+        and heads // n_tp * (rows // 8) <= 2 * LANES
         and tokens.shape[1] // n_kv == heads * DK // n_tp
         and tokens.shape[1] % (n_kv * n_tp * 2 * LANES) == 0
         and heads * DK // n_tp % (4 * LANES) == 0

time: 49.9 us -> 46.2 us (0.926)
  Pallas kernels: 49.1 us -> 45.4 us
    pallas_call x1, Pallas kernels: 49.1 us -> 45.4 us  [fused(): pl.pallas_call(functools.partial(layer_kernel, n_kv, n_tp), out_shape=plt...]
where the time goes in v2:
time: 46.2 us; the launch traced here: 46 us
  Pallas kernels  45.4 us (98%)
  local copies, waits for them, and re-layouts  0.6 us (1%)
    pallas_call x1, Pallas kernels, fused(): pl.pallas_call(functools.partial(layer_kernel, n_kv, n_tp), out_shape=plt...  45.4 us

profile of v2, /device:TPU:0, one launch (start us, length us, event | category | flops | bytes accessed | tf_op | source)
XLA Modules:
  0.0 46.0 jit_solution(15779542859056459864)
XLA Ops:
  0.0 45.4 %shard_map.154 = bf16[24,256]{1,0:T(8,128)(2,1)S(1)} custom-call(bf16[24,256]{1,0:T(8,128)(2,1)} %tokens_hbm.1, s32[24]{0:T(128)} %lengths_hbm.1, f32[1,1024]{1,0:T(1,128)} %bitcast.3, f32[4]{0:T(128)} %log_decay_hbm.1, f32[1,1024]{1,0:T(1,128)} %bitcast.4, f32[1,1024]{1,0:T(1,128)} %bitcast.5, bf16[1024,1024]{1,0:T(8,128)(2,1)} %wq_hbm.1, ...), custom_call_target="tpu_custom_call" | custom-call | tf_op jit(solution)/shard_map/pallas_call | solution.py:827
  45.4 0.6 %copy.18 = bf16[24,256]{1,0:T(8,128)(2,1)} copy(bf16[24,256]{1,0:T(8,128)(2,1)S(1)} %shard_map.154) | data formatting | bytes 24576

commit v3 on v2

v3 whole, which is shorter than its diff:
```python
import functools
import math

import jax
import jax.numpy as jnp
from jax import lax
from jax.experimental import pallas as pl
from jax.experimental.pallas import tpu as pltpu
from jax.sharding import PartitionSpec as P

DK = 256
D = 4096


RMS_EPS = 0.1
GN_EPS = 1.0
ROPE_BASE = 10000.0


def rotate(vectors, positions):
    half_dim = vectors.shape[-1] // 2
    inverse = ROPE_BASE ** (-jnp.arange(half_dim, dtype=jnp.float32) / half_dim)
    angles = positions[:, None, None] * inverse[None, None, :]
    cosine = jnp.cos(angles)
    sine_part = jnp.sin(angles)
    front_part = vectors[..., :half_dim]
    back_part = vectors[..., half_dim:]
    return jnp.concatenate(
        [front_part * cosine - back_part * sine_part, front_part * sine_part + back_part * cosine],
        axis=-1,
    )


def group_norm(totals, gn_gain):
    width = totals.shape[-1]
    center = jnp.sum(totals, axis=-1, keepdims=True) / width
    spread = jnp.sum(totals * totals, axis=-1, keepdims=True) / width - center * center
    normed = (totals - center) * lax.rsqrt(spread + GN_EPS)
    return normed.reshape(normed.shape[0], -1) * gn_gain


def channel_stat(own_squares):
    return lax.psum(own_squares, "kv")


def input_stat(own_squares):
    return lax.psum(own_squares, "kv")


def cache_partial(query_low, lengths, log_decay, key_cache, value_cache, heads_here):
    batch_rows = query_low.shape[0]
    span = key_cache.shape[1]
    slots = lax.axis_index("kv") * span + jnp.arange(span, dtype=jnp.int32)
    live = slots[None, :] < lengths[:, None]
    gaps = jnp.maximum((lengths[:, None] - slots[None, :]).astype(jnp.float32), 0.0)
    decays = jnp.exp(log_decay[None, None, :] * gaps[:, :, None])
    keys_here = key_cache.reshape(batch_rows, span, heads_here, DK)
    values_here = value_cache.reshape(batch_rows, span, heads_here, DK)
    scores = jnp.einsum("bphd,bhd->bph", keys_here, query_low, preferred_element_type=jnp.float32)
    mixing = jnp.where(live[:, :, None], scores * decays, 0.0).astype(jnp.bfloat16)
    return jnp.einsum("bph,bphd->bhd", mixing, values_here, preferred_element_type=jnp.float32)


def local(
    tokens,
    lengths,
    attn_gain,
    w_query,
    w_key,
    w_value,
    w_gate,
    log_decay,
    key_cache,
    value_cache,
    gn_gain,
    w_out,
    ffn_gain,
    w_ffn_gate,
    w_ffn_up,
    w_ffn_down,
):
    batch_rows = tokens.shape[0]
    heads_here = log_decay.shape[0]
    row_block = lax.all_gather(tokens, "tp", axis=1, tiled=True)
    widened = row_block.astype(jnp.float32)
    own_squares = jnp.sum(widened * widened, axis=1)
    scaled = (widened * attn_gain).astype(jnp.bfloat16)
    part_query = jnp.dot(scaled, w_query, preferred_element_type=jnp.float32)
    part_key = jnp.dot(scaled, w_key, preferred_element_type=jnp.float32)
    part_value = jnp.dot(scaled, w_value, preferred_element_type=jnp.float32)
    part_gate = jnp.dot(scaled, w_gate, preferred_element_type=jnp.float32)
    positions = lengths.astype(jnp.float32)
    total_squares = input_stat(own_squares)
    queries, new_keys, new_values, gates = lax.psum(
        (part_query, part_key, part_value, part_gate), "kv"
    )
    factor = lax.rsqrt(total_squares / D + RMS_EPS)[:, None]
    queries = rotate((queries * factor).reshape(batch_rows, heads_here, DK), positions) * DK ** (
        -0.5
    )
    new_keys = rotate((new_keys * factor).reshape(batch_rows, heads_here, DK), positions)
    new_values = (new_values * factor).reshape(batch_rows, heads_here, DK)
    gates = gates * factor
    query_low = queries.astype(jnp.bfloat16)
    partial_value = cache_partial(query_low, lengths, log_decay, key_cache, value_cache, heads_here)
    cached = lax.psum(partial_value.reshape(batch_rows, heads_here * DK), "kv")
    own_term = jnp.sum(queries * new_keys, axis=-1, keepdims=True) * new_values
    normed = group_norm(cached.reshape(batch_rows, heads_here, DK) + own_term, gn_gain)
    gated = (jax.nn.silu(gates) * normed).astype(jnp.bfloat16)
    out_partial = jnp.dot(gated, w_out, preferred_element_type=jnp.float32)
    mixed = lax.psum_scatter(out_partial, "tp", scatter_dimension=1, tiled=True)
    resid = (tokens.astype(jnp.float32) + mixed).astype(jnp.bfloat16)
    resid_block = lax.all_gather(resid, "tp", axis=1, tiled=True).astype(jnp.float32)
    mid_squares = jnp.sum(resid_block * resid_block, axis=1)
    scaled_mid = (resid_block * ffn_gain).astype(jnp.bfloat16)
    gate_part = jnp.dot(scaled_mid, w_ffn_gate, preferred_element_type=jnp.float32)
    up_part = jnp.dot(scaled_mid, w_ffn_up, preferred_element_type=jnp.float32)
    total_mid = channel_stat(mid_squares)
    gate_sum, up_sum = lax.psum((gate_part, up_part), "kv")
    factor_mid = lax.rsqrt(total_mid / D + RMS_EPS)[:, None]
    hidden = (jax.nn.silu(gate_sum * factor_mid) * (up_sum * factor_mid)).astype(jnp.bfloat16)
    down_partial = jnp.dot(hidden, w_ffn_down, preferred_element_type=jnp.float32)
    down = lax.psum_scatter(down_partial, "tp", scatter_dimension=1, tiled=True)
    return (resid.astype(jnp.float32) + down).astype(jnp.bfloat16)


LANES = 128
STAGE_TILES = 2
VG_AFTER = 1
F32 = jnp.float32
BF16 = jnp.bfloat16


def partner(index, j, parts):
    found, bit = 0, 1
    while bit < parts:
        digit = (index // bit) % 2
        found = found + bit * ((1 - digit) if (j // bit) % 2 else digit)
        bit *= 2
    return found


def stack(value, pieces):
    width = value.shape[1] // pieces
    return jnp.concatenate(
        [value[:, i * width : (i + 1) * width] for i in range(pieces)], axis=0
    ).astype(BF16)


def unstack(packed, pieces):
    wide = packed.astype(F32)
    rows = wide.shape[0] // pieces
    return jnp.concatenate([wide[i * rows : (i + 1) * rows] for i in range(pieces)], axis=1)


def pack(value):
    return stack(value, 2)


def unpack(packed):
    return unstack(packed, 2)


def plan(tiles, n_kv):
    step = STAGE_TILES * n_kv
    return tiles // step, tiles % step


def layer_kernel(
    n_kv,
    n_tp,
    tokens_hbm,
    lengths_hbm,
    attn_gain_hbm,
    log_decay_hbm,
    gn_gain_hbm,
    ffn_gain_hbm,
    wq_hbm,
    wk_hbm,
    wv_hbm,
    wg_hbm,
    kc_hbm,
    vc_hbm,
    wo_hbm,
    wfg_hbm,
    wfu_hbm,
    wfd_hbm,
    out_ref,
    wq,
    wk,
    wv,
    wg,
    kc,
    vc,
    wo,
    wfg,
    wfu,
    wfd,
    tokens_ref,
    lengths_ref,
    attn_gain_ref,
    log_decay_ref,
    gn_gain_ref,
    ffn_gain_ref,
    tok_buf,
    x_buf,
    sq_send,
    sq_recv,
    q_send,
    q_recv,
    q_full,
    trig,
    decay_buf,
    key_own,
    vg_send,
    vg_in,
    ca_send,
    ca_in,
    sc_send,
    sc_in,
    gt_send,
    gt_buf,
    o_buf,
    resid_buf,
    sqm_send,
    sqm_recv,
    gu_own,
    gu_send,
    gu_recv,
    hid_send,
    hid_recv,
    rest_send,
    rest_recv,
    rest_hid,
    down_buf,
    d_send,
    d_recv,
    load_sem,
    send_sem,
    recv_sem,
):
    rows, own_cols = tokens_ref.shape
    depth, wide = wq.shape
    span = kc.shape[1]
    half = DK // 2
    tiles = wfg.shape[1] // LANES
    win = STAGE_TILES * LANES
    n_full, rest = plan(tiles, n_kv)
    rest_tiles = rest // 2
    rest_base = n_full * STAGE_TILES * n_kv * LANES
    heads = n_kv
    middle = n_kv // 2 - 1
    shared = heads // 2
    me_kv = lax.axis_index("kv")
    me_tp = lax.axis_index("tp")
    me_core = me_tp % 2
    first_core = me_tp - me_core
    is_middle = (me_kv >= middle) & (me_kv < middle + 2)
    is_owner = (me_core == 1) & is_middle

    def kv_peer(j):
        return partner(me_kv, j, n_kv)

    def tp_peer(j):
        return partner(me_tp, j, n_tp)

    kv_order = tuple(range(n_kv - 1, 0, -1))

    barrier = pltpu.get_barrier_semaphore()
    for j in range(1, n_kv):
        for places in ({"kv": kv_peer(j)}, {"kv": kv_peer(j), "tp": tp_peer(1)}):
            pl.semaphore_signal(
                barrier, inc=1, device_id=places, device_id_type=pl.DeviceIdType.MESH
            )
    for j in range(1, n_tp):
        pl.semaphore_signal(
            barrier, inc=1, device_id={"tp": tp_peer(j)}, device_id_type=pl.DeviceIdType.MESH
        )

    loads = {}
    for slot, (name, src, dst) in enumerate(
        (
            ("tok", tokens_hbm, tokens_ref),
            ("len", lengths_hbm, lengths_ref),
            ("ag", attn_gain_hbm, attn_gain_ref),
            ("ld", log_decay_hbm, log_decay_ref),
            ("gg", gn_gain_hbm, gn_gain_ref),
            ("fg", ffn_gain_hbm, ffn_gain_ref),
            ("wq", wq_hbm, wq),
            ("kc", kc_hbm, kc),
            ("vc", vc_hbm, vc),
            ("wk", wk_hbm, wk),
            ("wv", wv_hbm, wv),
            ("wg", wg_hbm, wg),
            ("wo", wo_hbm, wo),
            ("wfg", wfg_hbm, wfg),
            ("wfu", wfu_hbm, wfu),
            ("wfd", wfd_hbm, wfd),
        )
    ):
        loads[name] = pltpu.make_async_copy(src, dst, load_sem.at[slot])

    names = ["tok", "sq", "q", "o", "sqm", "gu", "hid", "d", "gt", "rhid"]
    names += [f"{kind}{i}" for kind in ("vg", "ca", "sc", "rest") for i in range(2)]
    out_slot = {name: i for i, name in enumerate(names)}
    names = ["tok", "sq", "vg", "ca", "sc", "gt0", "gt1", "o0", "o1", "sqm", "d"]
    names += [f"q{h}" for h in range(heads)] + ["rest", "rhid0", "rhid1"]
    names += [f"{kind}{i}" for kind in ("gu", "hid") for i in range(n_full)]
    in_slot = {name: i for i, name in enumerate(names)}

    def remote(out, into, src, dst, where):
        return pltpu.make_async_remote_copy(
            src_ref=src,
            dst_ref=dst,
            send_sem=send_sem.at[out_slot[out]],
            recv_sem=recv_sem.at[in_slot[into]],
            device_id=where,
            device_id_type=pl.DeviceIdType.MESH,
        )

    def wait_in(into, ref):
        remote("tok", into, ref, ref, {"kv": kv_peer(1)}).wait_recv()

    def wait_out(out, ref):
        remote(out, "tok", ref, ref, {"kv": kv_peer(1)}).wait_send()

    def to_tp(out, into, src_of, dst):
        for chip in range(n_tp // 2 - 1, 0, -1):
            for core in (0, 1):
                target = partner(first_core, 2 * chip, n_tp) + core
                remote(out, into, src_of(target), dst, {"tp": target}).start()
        remote(out, into, src_of(tp_peer(1)), dst, {"tp": tp_peer(1)}).start()

    def column_tile(columns):
        lane_id = lax.broadcasted_iota(jnp.int32, (8, LANES), 1)
        tile = jnp.zeros((8, LANES), F32)
        groups = rows // 8
        for i, column in enumerate(columns):
            for r in range(groups):
                part = jnp.broadcast_to(column[r * 8 : (r + 1) * 8], (8, LANES))
                tile = jnp.where(lane_id == i * groups + r, part, tile)
        return tile

    def tile_column(tile, i):
        groups = rows // 8
        return jnp.concatenate(
            [tile[:, i * groups + r : i * groups + r + 1] for r in range(groups)], axis=0
        )

    for name in ("tok", "len", "ld", "ag", "wq"):
        loads[name].start()
    loads["tok"].wait()
    pl.semaphore_wait(barrier, 2 * (n_kv - 1) + n_tp - 1)

    to_tp("tok", "tok", lambda target: tokens_ref, tok_buf.at[me_tp])
    for name in ("wk", "wv", "wg", "kc", "vc", "gg", "fg"):
        loads[name].start()
    tok_buf[me_tp] = tokens_ref[...]

    for name in ("len", "ld", "ag"):
        loads[name].wait()
    row_id = lax.broadcasted_iota(jnp.int32, (rows, LANES), 0)
    lens = jnp.zeros((rows, LANES), jnp.int32)
    for b in range(rows):
        lens = jnp.where(row_id == b, lengths_ref[b], lens)
    lane = lax.broadcasted_iota(jnp.int32, (rows, half), 1).astype(F32)
    inverse = jnp.exp(lane * (-math.log(ROPE_BASE) / half))
    angles = lens[:, :1].astype(F32) * inverse
    trig[0] = jnp.cos(angles)
    trig[1] = jnp.sin(angles)
    places = rows * span
    col = lax.broadcasted_iota(jnp.int32, (rows, places), 1)
    row = lax.broadcasted_iota(jnp.int32, (rows, places), 0)
    slot = col - row * span
    position = slot + me_kv * span
    gap = lens[:, :1] - position
    live = (slot >= 0) & (slot < span) & (gap > 0)
    gap_f = jnp.where(live, gap, 0).astype(F32)
    for h in range(heads):
        decay_buf[h] = jnp.where(live, jnp.exp(gap_f * log_decay_ref[h]), 0.0)

    def rotate_in(front, back):
        cosine, sine = trig[0], trig[1]
        return front * cosine - back * sine, front * sine + back * cosine

    wait_in("tok", tok_buf.at[pl.ds(0, n_tp - 1)])
    squares = jnp.zeros((rows, 1), F32)
    for c in range(n_tp):
        wide_tok = tok_buf[c].astype(F32)
        squares = squares + jnp.sum(wide_tok * wide_tok, axis=1, keepdims=True)
        cols = pl.ds(c * own_cols, own_cols)
        x_buf[:, cols] = (wide_tok * attn_gain_ref[:, cols]).astype(BF16)
    sq_send[...] = column_tile([squares])
    for j in kv_order:
        remote("sq", "sq", sq_send, sq_recv.at[j - 1], {"kv": kv_peer(j)}).start()

    x = x_buf[...]
    loads["wq"].wait()
    for pair in range(heads // 2):
        q_own = jnp.dot(x, wq[:, pl.ds(pair * 2 * DK, 2 * DK)], preferred_element_type=F32)
        for i in range(2):
            h = pair * 2 + i
            piece = q_own[:, i * DK : (i + 1) * DK]
            q_send[h] = pack(piece)
            q_full[:, pl.ds(h * DK, DK)] = piece
            for j in kv_order:
                remote(
                    "q", f"q{h}", q_send.at[h], q_recv.at[h, j - 1], {"kv": kv_peer(j)}
                ).start()
    for name in ("wo", "wfg", "wfu", "wfd"):
        loads[name].start()

    for name in ("wk", "wv", "wg"):
        loads[name].wait()
    for i, weight in enumerate((wv, wg)):
        for pair in range(heads // 2):
            part = jnp.dot(x, weight[:, pl.ds(pair * 2 * DK, 2 * DK)], preferred_element_type=F32)
            for k in range(2):
                vg_send[pair * 2 + k, i] = pack(part[:, k * DK : (k + 1) * DK])
    key_own[...] = jnp.dot(x, wk[...], preferred_element_type=F32)

    wait_in("sq", sq_recv)
    total_sq = sq_send[...]
    for j in range(1, n_kv):
        total_sq = total_sq + sq_recv[j - 1]
    factor = lax.rsqrt(tile_column(total_sq, 0) / D + RMS_EPS)

    loads["kc"].wait()
    loads["vc"].wait()

    def owner_slot(oi):
        apart = partner(me_kv, middle + oi, n_kv)
        return jnp.where(me_core == 0, me_kv, n_kv - 1 + apart)

    def to_owner(oi, copies):
        @pl.when(jnp.logical_not((me_core == 1) & (me_kv == middle + oi)))
        def _():
            for kind, src, dst in copies:
                where = {"kv": middle + oi, "tp": first_core + 1}
                remote(f"{kind}{oi}", kind, src, dst, where).start()

    own_scores = []
    for h in range(heads):
        cols = pl.ds(h * DK, DK)
        wait_in(f"q{h}", q_recv.at[h])
        query = q_full[:, cols]
        for j in kv_order:
            query = query + unpack(q_recv[h, j - 1])
        query = query * factor
        front, back = rotate_in(query[:, :half], query[:, half:])
        query = jnp.concatenate([front, back], axis=1) * DK ** (-0.5)
        scores = lax.dot_general(
            query.astype(BF16),
            kc[:, :, cols].reshape(places, DK),
            (((1,), (1,)), ((), ())),
            preferred_element_type=F32,
        )
        mixing = (scores * decay_buf[h]).astype(BF16)
        cached = jnp.dot(mixing, vc[:, :, cols].reshape(places, DK), preferred_element_type=F32)
        ca_send[h] = pack(cached)
        key = key_own[:, cols]
        front, back = rotate_in(key[:, :half], key[:, half:])
        own_scores.append(
            jnp.sum(query[:, :half] * front + query[:, half:] * back, axis=1, keepdims=True)
            * factor
        )
        oi, hh = h // shared, h % shared
        copies = [("ca", ca_send.at[h], ca_in.at[owner_slot(oi), hh])]
        if hh == shared - 1:
            sc_send[oi] = column_tile(own_scores[oi * shared :])
            copies.append(("sc", sc_send.at[oi], sc_in.at[owner_slot(oi)]))
        to_owner(oi, copies)
        if h == VG_AFTER:
            for i in range(2):
                group = vg_send.at[pl.ds(i * shared, shared)]
                to_owner(i, [("vg", group, vg_in.at[owner_slot(i)])])

    @pl.when(is_owner)
    def _():
        oi = me_kv - middle
        base = oi * shared
        units = [(c, hh) for c in (1, 0) for hh in range(shared)]
        slots = {0: range(n_kv), 1: range(n_kv, 2 * n_kv - 1)}
        wait_in("vg", vg_in)
        gates, news = {}, {}
        for c, hh in units:
            parts = [[vg_in[k, hh, i] for k in slots[c]] for i in range(2)]
            if c:
                parts = [[vg_send[base + hh, i]] + parts[i] for i in range(2)]
            both = []
            for i in range(2):
                total = unpack(parts[i][0])
                for part in parts[i][1:]:
                    total = total + unpack(part)
                both.append(total * factor)
            news[c, hh] = both[0]
            gates[c, hh] = both[1] / (1.0 + jnp.exp(-both[1]))
        wait_in("sc", sc_in)
        wait_in("ca", ca_in)
        tiles_of = {}
        for c in (0, 1):
            parts = [sc_in[k] for k in slots[c]] + ([sc_send[oi]] if c else [])
            tiles_of[c] = functools.reduce(lambda p, q: p + q, parts)
        totals = {}
        for c, hh in units:
            total = tile_column(tiles_of[c], hh) * news[c, hh]
            if c:
                total = total + unpack(ca_send[base + hh])
            for k in slots[c]:
                total = total + unpack(ca_in[k, hh])
            totals[c, hh] = total
        sums = {u: jnp.sum(totals[u], axis=1, keepdims=True) for u in units}
        squared = {u: jnp.sum(totals[u] * totals[u], axis=1, keepdims=True) for u in units}
        for c, hh in units:
            center = sums[c, hh] / DK
            spread = squared[c, hh] / DK - center * center
            normed = (totals[c, hh] - center) * lax.rsqrt(spread + GN_EPS)
            result = pack(gates[c, hh] * normed)
            gt_send[c, hh] = result
            if c:
                gt_buf[oi, hh] = result
        for c in (0, 1):
            for j in kv_order + ((0,) if c == 0 else ()):
                where = {"kv": kv_peer(j) if j else me_kv, "tp": first_core + c}
                for i in range(2):

                    @pl.when(oi == i)
                    def _():
                        remote("gt", f"gt{i}", gt_send.at[c], gt_buf.at[i], where).start()

    loads["wo"].wait()
    loads["gg"].wait()
    for i in range(2):

        @pl.when(jnp.logical_not((me_core == 1) & (me_kv == middle + i)))
        def _():
            wait_in(f"gt{i}", gt_buf.at[i])

    for h in range(heads):
        cols = pl.ds(h * DK, DK)
        x_buf[:, cols] = (
            unpack(gt_buf[h // shared, h % shared]) * gn_gain_ref[:, cols]
        ).astype(BF16)
    gated = x_buf[...]
    for part in range(2):
        width = depth // 2
        piece = jnp.dot(gated, wo[:, pl.ds(part * width, width)], preferred_element_type=F32)
        o_buf[part, me_tp] = pack(piece)
        to_tp("o", f"o{part}", lambda target: o_buf.at[part, me_tp], o_buf.at[part, me_tp])
    loads["fg"].wait()
    for part in range(2):
        wait_in(f"o{part}", o_buf.at[part, pl.ds(0, n_tp - 1)])
    squares = jnp.zeros((rows, 1), F32)
    halves = []
    for part in range(2):
        total = unpack(o_buf[part, 0])
        for t in range(1, n_tp):
            total = total + unpack(o_buf[part, t])
        halves.append(total)
    mixed = jnp.concatenate(halves, axis=1)
    for c in range(n_tp):
        cols = pl.ds(c * own_cols, own_cols)
        own_mixed = mixed[:, c * own_cols : (c + 1) * own_cols]
        resid = (tok_buf[c].astype(F32) + own_mixed).astype(BF16)
        resid_wide = resid.astype(F32)
        resid_buf[c] = resid_wide
        squares = squares + jnp.sum(resid_wide * resid_wide, axis=1, keepdims=True)
        x_buf[:, cols] = (resid_wide * ffn_gain_ref[:, cols]).astype(BF16)
    sqm_send[...] = column_tile([squares])
    for j in kv_order:
        remote("sqm", "sqm", sqm_send, sqm_recv.at[j - 1], {"kv": kv_peer(j)}).start()

    x = x_buf[...]
    loads["wfg"].wait()
    loads["wfu"].wait()

    def stage_start(s, index):
        return pl.multiple_of((s * n_kv + index) * win, win)

    for s in range(n_full):
        for j in kv_order:
            cols = pl.ds(stage_start(s, kv_peer(j)), win)
            for i, weight in enumerate((wfg, wfu)):
                part = jnp.dot(x, weight[:, cols], preferred_element_type=F32)
                gu_send[s, j - 1, i] = pack(part)
            remote(
                "gu", f"gu{s}", gu_send.at[s, j - 1], gu_recv.at[s, j - 1], {"kv": kv_peer(j)}
            ).start()
    if rest:
        cols = pl.ds(rest_base, rest * LANES)
        both = [jnp.dot(x, w[:, cols], preferred_element_type=F32) for w in (wfg, wfu)]
        width = rest_tiles * LANES
        for o in range(2):
            mine = jnp.concatenate([b[:, o * width : (o + 1) * width] for b in both], axis=1)
            rest_send[o] = stack(mine, 2 * rest_tiles)
        for o in range(2):

            @pl.when(me_kv != middle + o)
            def _():
                apart = partner(me_kv, middle + o, n_kv)
                where = {"kv": middle + o}
                remote(
                    f"rest{o}", "rest", rest_send.at[o], rest_recv.at[apart - 1], where
                ).start()

    for s in range(n_full):
        cols = pl.ds(stage_start(s, me_kv), win)
        for i, weight in enumerate((wfg, wfu)):
            gu_own[s, i] = jnp.dot(x, weight[:, cols], preferred_element_type=F32)

    wait_in("sqm", sqm_recv)
    total_sq = sqm_send[...]
    for j in range(1, n_kv):
        total_sq = total_sq + sqm_recv[j - 1]
    factor = lax.rsqrt(tile_column(total_sq, 0) / D + RMS_EPS)

    def activate(gate, up):
        gate, up = gate * factor, up * factor
        return gate / (1.0 + jnp.exp(-gate)) * up

    for s in range(n_full):
        wait_in(f"gu{s}", gu_recv.at[s])
        both = []
        for i in range(2):
            total = gu_own[s, i]
            for j in kv_order:
                total = total + unpack(gu_recv[s, j - 1, i])
            both.append(total)
        hid_send[s] = pack(activate(*both))
        for j in kv_order:
            remote(
                "hid", f"hid{s}", hid_send.at[s], hid_recv.at[s, j - 1], {"kv": kv_peer(j)}
            ).start()

    if rest:

        @pl.when(is_middle)
        def _():
            o = me_kv - middle
            wait_in("rest", rest_recv)
            total = unstack(rest_send[o], 2 * rest_tiles)
            for k in range(n_kv - 1):
                total = total + unstack(rest_recv[k], 2 * rest_tiles)
            width = rest_tiles * LANES
            rest_hid[o] = stack(activate(total[:, :width], total[:, width:]), rest_tiles)
            for j in kv_order:
                for i in range(2):

                    @pl.when(o == i)
                    def _():
                        remote(
                            "rhid",
                            f"rhid{i}",
                            rest_hid.at[i],
                            rest_hid.at[i],
                            {"kv": kv_peer(j)},
                        ).start()

    loads["wfd"].wait()

    def down_of(s, index, packed):
        weight = wfd[pl.ds(stage_start(s, index), win), :]
        return jnp.dot(unpack(packed).astype(BF16), weight, preferred_element_type=F32)

    down = None
    for s in range(n_full):
        part = down_of(s, me_kv, hid_send[s])
        down = part if down is None else down + part
    for s in range(n_full):
        wait_in(f"hid{s}", hid_recv.at[s])
        for j in range(1, n_kv):
            down = down + down_of(s, kv_peer(j), hid_recv[s, j - 1])
    if rest:
        for o in range(2):

            @pl.when(me_kv != middle + o)
            def _():
                wait_in(f"rhid{o}", rest_hid.at[o])

        chunk = jnp.concatenate([unstack(rest_hid[o], rest_tiles) for o in range(2)], axis=1)
        weight = wfd[pl.ds(rest_base, rest * LANES), :]
        down = down + jnp.dot(chunk.astype(BF16), weight, preferred_element_type=F32)
    down_buf[...] = down
    for t in range(n_tp):
        d_send[t] = pack(down_buf[:, pl.ds(t * own_cols, own_cols)])
    to_tp("d", "d", lambda target: d_send.at[target], d_recv.at[me_tp])
    own = pl.ds(pl.multiple_of(me_tp * own_cols, own_cols), own_cols)
    result = down_buf[:, own] + resid_buf[me_tp]
    wait_in("d", d_recv.at[pl.ds(0, n_tp - 1)])
    for j in range(1, n_tp):
        result = result + unpack(d_recv[tp_peer(j)])
    out_ref[...] = result.astype(BF16)
    wait_out("tok", tok_buf.at[pl.ds(0, n_tp - 1)])
    wait_out("sq", sq_recv)
    wait_out("q", q_recv)
    wait_out("o", o_buf.at[:, pl.ds(0, n_tp - 1)])
    wait_out("sqm", sqm_recv)
    wait_out("gu", gu_recv)
    wait_out("hid", hid_recv)
    wait_out("d", d_recv.at[pl.ds(0, n_tp - 1)])
    for i in range(2):

        @pl.when(jnp.logical_not((me_core == 1) & (me_kv == middle + i)))
        def _():
            group = pl.ds(i * shared, shared)
            wait_out(f"vg{i}", vg_send.at[group])
            wait_out(f"ca{i}", ca_send.at[group])
            wait_out(f"sc{i}", sc_send.at[i])

        if rest:

            @pl.when(me_kv != middle + i)
            def _():
                wait_out(f"rest{i}", rest_send.at[i])

    @pl.when(is_owner)
    def _():
        wait_out("gt", ca_in)

    if rest:

        @pl.when(is_middle)
        def _():
            wait_out("rhid", rest_hid)


def fused(
    n_kv,
    n_tp,
    tokens,
    lengths,
    attn_gain,
    w_query,
    w_key,
    w_value,
    w_gate,
    log_decay,
    key_cache,
    value_cache,
    gn_gain,
    w_out,
    ffn_gain,
    w_ffn_gate,
    w_ffn_up,
    w_ffn_down,
):
    rows, own_cols = tokens.shape
    depth, wide = w_query.shape
    span = key_cache.shape[1]
    heads = log_decay.shape[0]
    shared = heads // 2
    win = STAGE_TILES * LANES
    n_full, rest = plan(w_ffn_gate.shape[1] // LANES, n_kv)
    rest_rows = max(rest // 2, 1) * rows
    peers = n_kv - 1
    vmem = pl.BlockSpec(memory_space=pltpu.VMEM)
    hbm = pl.BlockSpec(memory_space=pl.ANY)
    small = (
        tokens,
        lengths,
        attn_gain[None, :],
        log_decay,
        gn_gain[None, :],
        ffn_gain[None, :],
    )
    streamed = (
        w_query,
        w_key,
        w_value,
        w_gate,
        key_cache,
        value_cache,
        w_out,
        w_ffn_gate,
        w_ffn_up,
        w_ffn_down,
    )
    scratch = [pltpu.VMEM(a.shape, a.dtype) for a in streamed] + [
        (pltpu.SMEM if a.ndim == 1 else pltpu.VMEM)(a.shape, a.dtype) for a in small
    ]
    piece = (2 * rows, DK // 2)
    scratch += [
        pltpu.VMEM((n_tp, rows, own_cols), BF16),
        pltpu.VMEM((rows, depth), BF16),
        pltpu.VMEM((8, LANES), F32),
        pltpu.VMEM((peers, 8, LANES), F32),
        pltpu.VMEM((heads, *piece), BF16),
        pltpu.VMEM((heads, peers, *piece), BF16),
        pltpu.VMEM((rows, wide), F32),
        pltpu.VMEM((2, rows, DK // 2), F32),
        pltpu.VMEM((heads, rows, rows * span), F32),
        pltpu.VMEM((rows, wide), F32),
        pltpu.VMEM((heads, 2, *piece), BF16),
        pltpu.VMEM((2 * n_kv - 1, shared, 2, *piece), BF16),
        pltpu.VMEM((heads, *piece), BF16),
        pltpu.VMEM((2 * n_kv - 1, shared, *piece), BF16),
        pltpu.VMEM((2, 8, LANES), F32),
        pltpu.VMEM((2 * n_kv - 1, 8, LANES), F32),
        pltpu.VMEM((2, shared, *piece), BF16),
        pltpu.VMEM((2, shared, *piece), BF16),
        pltpu.VMEM((2, n_tp, 2 * rows, depth // 4), BF16),
        pltpu.VMEM((n_tp, rows, own_cols), F32),
        pltpu.VMEM((8, LANES), F32),
        pltpu.VMEM((peers, 8, LANES), F32),
        pltpu.VMEM((n_full, 2, rows, win), F32),
        pltpu.VMEM((n_full, peers, 2, 2 * rows, win // 2), BF16),
        pltpu.VMEM((n_full, peers, 2, 2 * rows, win // 2), BF16),
        pltpu.VMEM((n_full, 2 * rows, win // 2), BF16),
        pltpu.VMEM((n_full, peers, 2 * rows, win // 2), BF16),
        pltpu.VMEM((2, 2 * rest_rows, LANES), BF16),
        pltpu.VMEM((peers, 2 * rest_rows, LANES), BF16),
        pltpu.VMEM((peers, rest_rows, LANES), BF16),
        pltpu.VMEM((rows, depth), F32),
        pltpu.VMEM((n_tp, 2 * rows, own_cols // 2), BF16),
        pltpu.VMEM((n_tp, 2 * rows, own_cols // 2), BF16),
        pltpu.SemaphoreType.DMA((len(small) + len(streamed),)),
        pltpu.SemaphoreType.DMA((18,)),
        pltpu.SemaphoreType.DMA((14 + heads + 2 * n_full,)),
    ]
    return pl.pallas_call(
        functools.partial(layer_kernel, n_kv, n_tp),
        out_shape=pltpu.VMEM((rows, own_cols), BF16),
        in_specs=[hbm] * (len(small) + len(streamed)),
        out_specs=vmem,
        scratch_shapes=scratch,
        compiler_params=pltpu.CompilerParams(
            collective_id=0, has_side_effects=True, vmem_limit_bytes=60 * 1024 * 1024
        ),
    )(*small, *streamed)


def fits(mesh, tokens, log_decay, key_cache, w_query, w_ffn_gate):
    n_kv, n_tp, n_grp = mesh.shape["kv"], mesh.shape["tp"], mesh.shape["grp"]
    heads, span = log_decay.shape[0], key_cache.shape[1] // n_kv
    tiles = w_ffn_gate.shape[1] // n_tp // LANES
    rows = tokens.shape[0] // n_grp
    return (
        n_kv > 1
        and n_tp > 2
        and n_kv & (n_kv - 1) == 0
        and n_tp & (n_tp - 1) == 0
        and heads == n_kv * n_tp
        and heads // n_tp * (rows // 8) <= 2 * LANES
        and tokens.shape[1] // n_kv == heads * DK // n_tp
        and tokens.shape[1] % (n_kv * n_tp * 2 * LANES) == 0
        and heads * DK // n_tp % (4 * LANES) == 0
        and w_ffn_gate.shape[1] % (n_tp * LANES) == 0
        and plan(tiles, n_kv)[0] > 0
        and plan(tiles, n_kv)[1] % 2 == 0
        and n_kv > 2
        and tokens.shape[0] // n_grp % 8 == 0
        and span % 16 == 0
        and span <= 64
    )


def solution(mesh):
    specs = (
        P("grp", ("kv", "tp")),
        P("grp"),
        P("kv"),
        P("kv", "tp"),
        P("kv", "tp"),
        P("kv", "tp"),
        P("kv", "tp"),
        P("tp"),
        P("grp", "kv", "tp"),
        P("grp", "kv", "tp"),
        P("tp"),
        P("tp", "kv"),
        P("kv"),
        P("kv", "tp"),
        P("kv", "tp"),
        P("tp", "kv"),
    )

    def whole(*arrays):
        tokens, w_query, log_decay, key_cache = arrays[0], arrays[3], arrays[7], arrays[8]
        if fits(mesh, tokens, log_decay, key_cache, w_query, arrays[13]):
            body = functools.partial(fused, mesh.shape["kv"], mesh.shape["tp"])
        else:
            body = local
        return jax.shard_map(
            body,
            mesh=mesh,
            in_specs=specs,
            out_specs=P("grp", ("kv", "tp")),
            check_vma=False,
        )(*arrays)

    return whole
```

time: 46.2 us -> 42.8 us (0.926)
  Pallas kernels: 45.4 us -> 42 us
    pallas_call x1, Pallas kernels: 45.4 us -> 42 us  [fused(): pl.pallas_call(functools.partial(layer_kernel, n_kv, n_tp), out_shape=plt...]
where the time goes in v3:
time: 42.8 us; the launch traced here: 42.6 us
  Pallas kernels  42 us (98%)
  local copies, waits for them, and re-layouts  0.6 us (1%)
    pallas_call x1, Pallas kernels, fused(): pl.pallas_call(functools.partial(layer_kernel, n_kv, n_tp), out_shape=plt...  42 us

profile of v3, /device:TPU:0, one launch (start us, length us, event | category | flops | bytes accessed | tf_op | source)
XLA Modules:
  0.0 42.6 jit_solution(16906860889089760753)
XLA Ops:
  0.0 42.0 %shard_map.154 = bf16[24,256]{1,0:T(8,128)(2,1)S(1)} custom-call(bf16[24,256]{1,0:T(8,128)(2,1)} %tokens_hbm.1, s32[24]{0:T(128)} %lengths_hbm.1, f32[1,1024]{1,0:T(1,128)} %bitcast.3, f32[4]{0:T(128)} %log_decay_hbm.1, f32[1,1024]{1,0:T(1,128)} %bitcast.4, f32[1,1024]{1,0:T(1,128)} %bitcast.5, bf16[1024,1024]{1,0:T(8,128)(2,1)} %wq_hbm.1, ...), custom_call_target="tpu_custom_call" | custom-call | tf_op jit(solution)/shard_map/pallas_call | solution.py:820
  42.0 0.6 %copy.18 = bf16[24,256]{1,0:T(8,128)(2,1)} copy(bf16[24,256]{1,0:T(8,128)(2,1)S(1)} %shard_map.154) | data formatting | bytes 24576

commit v4 on v3

--- a/solution.py
+++ b/solution.py
@@ -204,8 +204,6 @@
     ffn_gain_ref,
     tok_buf,
     x_buf,
-    sq_send,
-    sq_recv,
     q_send,
     q_recv,
     q_full,
@@ -231,6 +229,7 @@
     hid_recv,
     rest_send,
     rest_recv,
+    rest_out,
     rest_hid,
     down_buf,
     d_send,
@@ -238,6 +237,7 @@
     load_sem,
     send_sem,
     recv_sem,
+    go_sem,
 ):
     rows, own_cols = tokens_ref.shape
     depth, wide = wq.shape
@@ -267,15 +267,17 @@
     kv_order = tuple(range(n_kv - 1, 0, -1))
 
     barrier = pltpu.get_barrier_semaphore()
-    for j in range(1, n_kv):
-        for places in ({"kv": kv_peer(j)}, {"kv": kv_peer(j), "tp": tp_peer(1)}):
-            pl.semaphore_signal(
-                barrier, inc=1, device_id=places, device_id_type=pl.DeviceIdType.MESH
-            )
     for j in range(1, n_tp):
         pl.semaphore_signal(
             barrier, inc=1, device_id={"tp": tp_peer(j)}, device_id_type=pl.DeviceIdType.MESH
         )
+    for k in range(1, n_kv):
+
+        @pl.when(me_kv < k)
+        def _():
+            pl.semaphore_signal(
+                barrier, inc=1, device_id={"kv": k}, device_id_type=pl.DeviceIdType.MESH
+            )
 
     loads = {}
     for slot, (name, src, dst) in enumerate(
@@ -300,10 +302,10 @@
     ):
         loads[name] = pltpu.make_async_copy(src, dst, load_sem.at[slot])
 
-    names = ["tok", "sq", "q", "o", "sqm", "gu", "hid", "d", "gt", "rhid"]
+    names = ["tok", "q", "o", "sqm", "gu", "hid", "d", "gt", "rhid"]
     names += [f"{kind}{i}" for kind in ("vg", "ca", "sc", "rest") for i in range(2)]
     out_slot = {name: i for i, name in enumerate(names)}
-    names = ["tok", "sq", "vg", "ca", "sc", "gt0", "gt1", "o0", "o1", "sqm", "d"]
+    names = ["tok", "vg", "ca", "sc", "gt0", "gt1", "o0", "o1", "sqm", "d"]
     names += [f"q{h}" for h in range(heads)] + ["rest", "rhid0", "rhid1"]
     names += [f"{kind}{i}" for kind in ("gu", "hid") for i in range(n_full)]
     in_slot = {name: i for i, name in enumerate(names)}
@@ -331,27 +333,43 @@
                 remote(out, into, src_of(target), dst, {"tp": target}).start()
         remote(out, into, src_of(tp_peer(1)), dst, {"tp": tp_peer(1)}).start()
 
-    def column_tile(columns):
-        lane_id = lax.broadcasted_iota(jnp.int32, (8, LANES), 1)
-        tile = jnp.zeros((8, LANES), F32)
-        groups = rows // 8
+    lane_id = lax.broadcasted_iota(jnp.int32, (8, LANES), 1)
+    row_of = lax.broadcasted_iota(jnp.int32, (8, LANES), 0)
+
+    def lanes_of(columns):
+        spread = jnp.zeros((8, LANES), F32)
         for i, column in enumerate(columns):
-            for r in range(groups):
-                part = jnp.broadcast_to(column[r * 8 : (r + 1) * 8], (8, LANES))
-                tile = jnp.where(lane_id == i * groups + r, part, tile)
-        return tile
-
-    def tile_column(tile, i):
-        groups = rows // 8
+            for first in range(0, rows, 8):
+                part = jnp.broadcast_to(column[first : first + 8], (8, LANES))
+                spread = jnp.where(lane_id == row_of + (i * rows + first), part, spread)
+        return jnp.sum(spread, axis=0, keepdims=True)
+
+    def column_of(line, i):
+        wide_line = jnp.broadcast_to(line, (8, LANES))
         return jnp.concatenate(
-            [tile[:, i * groups + r : i * groups + r + 1] for r in range(groups)], axis=0
+            [
+                jnp.sum(
+                    jnp.where(lane_id == row_of + (i * rows + first), wide_line, 0.0),
+                    axis=1,
+                    keepdims=True,
+                )
+                for first in range(0, rows, 8)
+            ],
+            axis=0,
         )
 
     for name in ("tok", "len", "ld", "ag", "wq"):
         loads[name].start()
+    pl.semaphore_wait(barrier, n_tp - 1 + me_kv)
+    for k in range(n_kv - 1):
+
+        @pl.when(me_kv > k)
+        def _():
+            pl.semaphore_signal(
+                go_sem, inc=1, device_id={"kv": k}, device_id_type=pl.DeviceIdType.MESH
+            )
+
     loads["tok"].wait()
-    pl.semaphore_wait(barrier, 2 * (n_kv - 1) + n_tp - 1)
-
     to_tp("tok", "tok", lambda target: tokens_ref, tok_buf.at[me_tp])
     for name in ("wk", "wv", "wg", "kc", "vc", "gg", "fg"):
         loads[name].start()
@@ -390,9 +408,10 @@
         squares = squares + jnp.sum(wide_tok * wide_tok, axis=1, keepdims=True)
         cols = pl.ds(c * own_cols, own_cols)
         x_buf[:, cols] = (wide_tok * attn_gain_ref[:, cols]).astype(BF16)
-    sq_send[...] = column_tile([squares])
-    for j in kv_order:
-        remote("sq", "sq", sq_send, sq_recv.at[j - 1], {"kv": kv_peer(j)}).start()
+    @pl.when(me_kv < n_kv - 1)
+    def _():
+        pl.semaphore_wait(go_sem, n_kv - 1 - me_kv)
+
 
     x = x_buf[...]
     loads["wq"].wait()
@@ -419,12 +438,6 @@
                 vg_send[pair * 2 + k, i] = pack(part[:, k * DK : (k + 1) * DK])
     key_own[...] = jnp.dot(x, wk[...], preferred_element_type=F32)
 
-    wait_in("sq", sq_recv)
-    total_sq = sq_send[...]
-    for j in range(1, n_kv):
-        total_sq = total_sq + sq_recv[j - 1]
-    factor = lax.rsqrt(tile_column(total_sq, 0) / D + RMS_EPS)
-
     loads["kc"].wait()
     loads["vc"].wait()
 
@@ -446,7 +459,6 @@
         query = q_full[:, cols]
         for j in kv_order:
             query = query + unpack(q_recv[h, j - 1])
-        query = query * factor
         front, back = rotate_in(query[:, :half], query[:, half:])
         query = jnp.concatenate([front, back], axis=1) * DK ** (-0.5)
         scores = lax.dot_general(
@@ -462,12 +474,11 @@
         front, back = rotate_in(key[:, :half], key[:, half:])
         own_scores.append(
             jnp.sum(query[:, :half] * front + query[:, half:] * back, axis=1, keepdims=True)
-            * factor
         )
         oi, hh = h // shared, h % shared
         copies = [("ca", ca_send.at[h], ca_in.at[owner_slot(oi), hh])]
         if hh == shared - 1:
-            sc_send[oi] = column_tile(own_scores[oi * shared :])
+            sc_send[oi] = lanes_of(own_scores[oi * shared :] + [squares])
             copies.append(("sc", sc_send.at[oi], sc_in.at[owner_slot(oi)]))
         to_owner(oi, copies)
         if h == VG_AFTER:
@@ -481,6 +492,14 @@
         base = oi * shared
         units = [(c, hh) for c in (1, 0) for hh in range(shared)]
         slots = {0: range(n_kv), 1: range(n_kv, 2 * n_kv - 1)}
+        wait_in("sc", sc_in)
+        lines = {}
+        for c in (0, 1):
+            parts = [sc_in[k] for k in slots[c]] + ([sc_send[oi]] if c else [])
+            lines[c] = functools.reduce(lambda p, q: p + q, parts)
+        factor = lax.rsqrt(column_of(lines[1], shared) / D + RMS_EPS)
+        cubed = factor * factor * factor
+        weights = {u: column_of(lines[u[0]], u[1]) * cubed for u in units}
         wait_in("vg", vg_in)
         gates, news = {}, {}
         for c, hh in units:
@@ -492,23 +511,18 @@
                 total = unpack(parts[i][0])
                 for part in parts[i][1:]:
                     total = total + unpack(part)
-                both.append(total * factor)
-            news[c, hh] = both[0]
+                both.append(total)
+            news[c, hh] = weights[c, hh] * both[0]
+            both[1] = both[1] * factor
             gates[c, hh] = both[1] / (1.0 + jnp.exp(-both[1]))
-        wait_in("sc", sc_in)
         wait_in("ca", ca_in)
-        tiles_of = {}
-        for c in (0, 1):
-            parts = [sc_in[k] for k in slots[c]] + ([sc_send[oi]] if c else [])
-            tiles_of[c] = functools.reduce(lambda p, q: p + q, parts)
         totals = {}
         for c, hh in units:
-            total = tile_column(tiles_of[c], hh) * news[c, hh]
-            if c:
-                total = total + unpack(ca_send[base + hh])
-            for k in slots[c]:
-                total = total + unpack(ca_in[k, hh])
-            totals[c, hh] = total
+            parts = [ca_in[k, hh] for k in slots[c]] + ([ca_send[base + hh]] if c else [])
+            total = unpack(parts[0])
+            for part in parts[1:]:
+                total = total + unpack(part)
+            totals[c, hh] = total * factor + news[c, hh]
         sums = {u: jnp.sum(totals[u], axis=1, keepdims=True) for u in units}
         squared = {u: jnp.sum(totals[u] * totals[u], axis=1, keepdims=True) for u in units}
         for c, hh in units:
@@ -566,7 +580,7 @@
         resid_buf[c] = resid_wide
         squares = squares + jnp.sum(resid_wide * resid_wide, axis=1, keepdims=True)
         x_buf[:, cols] = (resid_wide * ffn_gain_ref[:, cols]).astype(BF16)
-    sqm_send[...] = column_tile([squares])
+    sqm_send[...] = lanes_of([squares])
     for j in kv_order:
         remote("sqm", "sqm", sqm_send, sqm_recv.at[j - 1], {"kv": kv_peer(j)}).start()
 
@@ -595,13 +609,7 @@
             rest_send[o] = stack(mine, 2 * rest_tiles)
         for o in range(2):
 
-            @pl.when(me_kv != middle + o)
-            def _():
-                apart = partner(me_kv, middle + o, n_kv)
-                where = {"kv": middle + o}
-                remote(
-                    f"rest{o}", "rest", rest_send.at[o], rest_recv.at[apart - 1], where
-                ).start()
+            to_owner(o, [("rest", rest_send.at[o], rest_recv.at[owner_slot(o)])])
 
     for s in range(n_full):
         cols = pl.ds(stage_start(s, me_kv), win)
@@ -612,7 +620,7 @@
     total_sq = sqm_send[...]
     for j in range(1, n_kv):
         total_sq = total_sq + sqm_recv[j - 1]
-    factor = lax.rsqrt(tile_column(total_sq, 0) / D + RMS_EPS)
+    factor = lax.rsqrt(column_of(total_sq, 0) / D + RMS_EPS)
 
     def activate(gate, up):
         gate, up = gate * factor, up * factor
@@ -634,27 +642,30 @@
 
     if rest:
 
-        @pl.when(is_middle)
+        @pl.when(is_owner)
         def _():
             o = me_kv - middle
             wait_in("rest", rest_recv)
-            total = unstack(rest_send[o], 2 * rest_tiles)
-            for k in range(n_kv - 1):
-                total = total + unstack(rest_recv[k], 2 * rest_tiles)
             width = rest_tiles * LANES
-            rest_hid[o] = stack(activate(total[:, :width], total[:, width:]), rest_tiles)
-            for j in kv_order:
-                for i in range(2):
-
-                    @pl.when(o == i)
-                    def _():
-                        remote(
-                            "rhid",
-                            f"rhid{i}",
-                            rest_hid.at[i],
-                            rest_hid.at[i],
-                            {"kv": kv_peer(j)},
-                        ).start()
+            for c in (0, 1):
+                slots = range(n_kv) if c == 0 else range(n_kv, 2 * n_kv - 1)
+                parts = [rest_recv[k] for k in slots] + ([rest_send[o]] if c else [])
+                total = unstack(parts[0], 2 * rest_tiles)
+                for part in parts[1:]:
+                    total = total + unstack(part, 2 * rest_tiles)
+                result = stack(activate(total[:, :width], total[:, width:]), rest_tiles)
+                rest_out[c] = result
+                if c:
+                    rest_hid[o] = result
+                for j in kv_order + ((0,) if c == 0 else ()):
+                    where = {"kv": kv_peer(j) if j else me_kv, "tp": first_core + c}
+                    for i in range(2):
+
+                        @pl.when(o == i)
+                        def _():
+                            remote(
+                                "rhid", f"rhid{i}", rest_out.at[c], rest_hid.at[i], where
+                            ).start()
 
     loads["wfd"].wait()
 
@@ -671,15 +682,22 @@
         for j in range(1, n_kv):
             down = down + down_of(s, kv_peer(j), hid_recv[s, j - 1])
     if rest:
-        for o in range(2):
-
-            @pl.when(me_kv != middle + o)
+        near = jnp.where(me_kv > middle, 1, 0)
+        width = rest_tiles * LANES
+        for o in (near, 1 - near):
+
+            @pl.when(jnp.logical_not((me_core == 1) & (me_kv == middle + o)))
             def _():
-                wait_in(f"rhid{o}", rest_hid.at[o])
-
-        chunk = jnp.concatenate([unstack(rest_hid[o], rest_tiles) for o in range(2)], axis=1)
-        weight = wfd[pl.ds(rest_base, rest * LANES), :]
-        down = down + jnp.dot(chunk.astype(BF16), weight, preferred_element_type=F32)
+                for i in range(2):
+
+                    @pl.when(o == i)
+                    def _():
+                        wait_in(f"rhid{i}", rest_hid.at[i])
+
+            chunk = unstack(rest_hid[o], rest_tiles).astype(BF16)
+            first = pl.multiple_of(rest_base + o * width, LANES)
+            weight = wfd[pl.ds(first, width), :]
+            down = down + jnp.dot(chunk, weight, preferred_element_type=F32)
     down_buf[...] = down
     for t in range(n_tp):
         d_send[t] = pack(down_buf[:, pl.ds(t * own_cols, own_cols)])
@@ -691,7 +709,6 @@
         result = result + unpack(d_recv[tp_peer(j)])
     out_ref[...] = result.astype(BF16)
     wait_out("tok", tok_buf.at[pl.ds(0, n_tp - 1)])
-    wait_out("sq", sq_recv)
     wait_out("q", q_recv)
     wait_out("o", o_buf.at[:, pl.ds(0, n_tp - 1)])
     wait_out("sqm", sqm_recv)
@@ -706,21 +723,13 @@
             wait_out(f"vg{i}", vg_send.at[group])
             wait_out(f"ca{i}", ca_send.at[group])
             wait_out(f"sc{i}", sc_send.at[i])
-
-        if rest:
-
-            @pl.when(me_kv != middle + i)
-            def _():
+            if rest:
                 wait_out(f"rest{i}", rest_send.at[i])
 
     @pl.when(is_owner)
     def _():
         wait_out("gt", ca_in)
-
-    if rest:
-
-        @pl.when(is_middle)
-        def _():
+        if rest:
             wait_out("rhid", rest_hid)
 
 
@@ -782,8 +791,6 @@
     scratch += [
         pltpu.VMEM((n_tp, rows, own_cols), BF16),
         pltpu.VMEM((rows, depth), BF16),
-        pltpu.VMEM((8, LANES), F32),
-        pltpu.VMEM((peers, 8, LANES), F32),
         pltpu.VMEM((heads, *piece), BF16),
         pltpu.VMEM((heads, peers, *piece), BF16),
         pltpu.VMEM((rows, wide), F32),
@@ -794,28 +801,30 @@
         pltpu.VMEM((2 * n_kv - 1, shared, 2, *piece), BF16),
         pltpu.VMEM((heads, *piece), BF16),
         pltpu.VMEM((2 * n_kv - 1, shared, *piece), BF16),
-        pltpu.VMEM((2, 8, LANES), F32),
-        pltpu.VMEM((2 * n_kv - 1, 8, LANES), F32),
+        pltpu.VMEM((2, 1, LANES), F32),
+        pltpu.VMEM((2 * n_kv - 1, 1, LANES), F32),
         pltpu.VMEM((2, shared, *piece), BF16),
         pltpu.VMEM((2, shared, *piece), BF16),
         pltpu.VMEM((2, n_tp, 2 * rows, depth // 4), BF16),
         pltpu.VMEM((n_tp, rows, own_cols), F32),
-        pltpu.VMEM((8, LANES), F32),
-        pltpu.VMEM((peers, 8, LANES), F32),
+        pltpu.VMEM((1, LANES), F32),
+        pltpu.VMEM((peers, 1, LANES), F32),
         pltpu.VMEM((n_full, 2, rows, win), F32),
         pltpu.VMEM((n_full, peers, 2, 2 * rows, win // 2), BF16),
         pltpu.VMEM((n_full, peers, 2, 2 * rows, win // 2), BF16),
         pltpu.VMEM((n_full, 2 * rows, win // 2), BF16),
         pltpu.VMEM((n_full, peers, 2 * rows, win // 2), BF16),
         pltpu.VMEM((2, 2 * rest_rows, LANES), BF16),
-        pltpu.VMEM((peers, 2 * rest_rows, LANES), BF16),
-        pltpu.VMEM((peers, rest_rows, LANES), BF16),
+        pltpu.VMEM((2 * n_kv - 1, 2 * rest_rows, LANES), BF16),
+        pltpu.VMEM((2, rest_rows, LANES), BF16),
+        pltpu.VMEM((2 * n_kv - 1, rest_rows, LANES), BF16),
         pltpu.VMEM((rows, depth), F32),
         pltpu.VMEM((n_tp, 2 * rows, own_cols // 2), BF16),
         pltpu.VMEM((n_tp, 2 * rows, own_cols // 2), BF16),
         pltpu.SemaphoreType.DMA((len(small) + len(streamed),)),
-        pltpu.SemaphoreType.DMA((18,)),
-        pltpu.SemaphoreType.DMA((14 + heads + 2 * n_full,)),
+        pltpu.SemaphoreType.DMA((17,)),
+        pltpu.SemaphoreType.DMA((13 + heads + 2 * n_full,)),
+        pltpu.SemaphoreType.REGULAR,
     ]
     return pl.pallas_call(
         functools.partial(layer_kernel, n_kv, n_tp),
@@ -840,7 +849,7 @@
         and n_kv & (n_kv - 1) == 0
         and n_tp & (n_tp - 1) == 0
         and heads == n_kv * n_tp
-        and heads // n_tp * (rows // 8) <= 2 * LANES
+        and (heads // n_tp // 2 + 1) * rows <= LANES
         and tokens.shape[1] // n_kv == heads * DK // n_tp
         and tokens.shape[1] % (n_kv * n_tp * 2 * LANES) == 0
         and heads * DK // n_tp % (4 * LANES) == 0

time: 42.8 us -> 40.8 us (0.953)
  Pallas kernels: 42 us -> 40.1 us
    pallas_call x1, Pallas kernels: 42 us -> 40.1 us  [fused(): pl.pallas_call(functools.partial(layer_kernel, n_kv, n_tp), out_shape=plt...]
where the time goes in v4:
time: 40.8 us; the launch traced here: 40.7 us
  Pallas kernels  40.1 us (98%)
  local copies, waits for them, and re-layouts  0.6 us (1%)
    pallas_call x1, Pallas kernels, fused(): pl.pallas_call(functools.partial(layer_kernel, n_kv, n_tp), out_shape=plt...  40.1 us

profile of v4, /device:TPU:0, one launch (start us, length us, event | category | flops | bytes accessed | tf_op | source)
XLA Modules:
  0.0 40.7 jit_solution(12696511729826133622)
XLA Ops:
  0.0 40.1 %shard_map.154 = bf16[24,256]{1,0:T(8,128)(2,1)S(1)} custom-call(bf16[24,256]{1,0:T(8,128)(2,1)} %tokens_hbm.1, s32[24]{0:T(128)} %lengths_hbm.1, f32[1,1024]{1,0:T(1,128)} %bitcast.3, f32[4]{0:T(128)} %log_decay_hbm.1, f32[1,1024]{1,0:T(1,128)} %bitcast.4, f32[1,1024]{1,0:T(1,128)} %bitcast.5, bf16[1024,1024]{1,0:T(8,128)(2,1)} %wq_hbm.1, ...), custom_call_target="tpu_custom_call" | custom-call | tf_op jit(solution)/shard_map/pallas_call | solution.py:829
  40.1 0.6 %copy.18 = bf16[24,256]{1,0:T(8,128)(2,1)} copy(bf16[24,256]{1,0:T(8,128)(2,1)S(1)} %shard_map.154) | data formatting | bytes 24576

commit v5 on v4

--- a/solution.py
+++ b/solution.py
@@ -126,7 +126,6 @@
 
 LANES = 128
 STAGE_TILES = 2
-VG_AFTER = 1
 F32 = jnp.float32
 BF16 = jnp.bfloat16
 
@@ -212,6 +211,8 @@
     key_own,
     vg_send,
     vg_in,
+    swap_send,
+    swap_recv,
     ca_send,
     ca_in,
     sc_send,
@@ -303,9 +304,10 @@
         loads[name] = pltpu.make_async_copy(src, dst, load_sem.at[slot])
 
     names = ["tok", "q", "o", "sqm", "gu", "hid", "d", "gt", "rhid"]
-    names += [f"{kind}{i}" for kind in ("vg", "ca", "sc", "rest") for i in range(2)]
+    names += [f"{kind}{i}" for kind in ("ca", "sc", "rest") for i in range(2)]
+    names += ["vg", "swap"]
     out_slot = {name: i for i, name in enumerate(names)}
-    names = ["tok", "vg", "ca", "sc", "gt0", "gt1", "o0", "o1", "sqm", "d"]
+    names = ["tok", "vg", "swap", "ca", "sc", "gt0", "gt1", "o0", "o1", "sqm", "d"]
     names += [f"q{h}" for h in range(heads)] + ["rest", "rhid0", "rhid1"]
     names += [f"{kind}{i}" for kind in ("gu", "hid") for i in range(n_full)]
     in_slot = {name: i for i, name in enumerate(names)}
@@ -436,6 +438,15 @@
             part = jnp.dot(x, weight[:, pl.ds(pair * 2 * DK, 2 * DK)], preferred_element_type=F32)
             for k in range(2):
                 vg_send[pair * 2 + k, i] = pack(part[:, k * DK : (k + 1) * DK])
+    side = jnp.where(me_kv > middle, 1, 0)
+    away = jnp.where(me_kv > middle, me_kv - middle - 1, middle - me_kv)
+
+    @pl.when(jnp.logical_not(is_owner))
+    def _():
+        slot = jnp.where(me_core == 0, away, n_kv // 2 - 1 + away)
+        where = {"kv": middle + side, "tp": first_core + 1}
+        remote("vg", "vg", vg_send, vg_in.at[slot], where).start()
+
     key_own[...] = jnp.dot(x, wk[...], preferred_element_type=F32)
 
     loads["kc"].wait()
@@ -481,10 +492,6 @@
             sc_send[oi] = lanes_of(own_scores[oi * shared :] + [squares])
             copies.append(("sc", sc_send.at[oi], sc_in.at[owner_slot(oi)]))
         to_owner(oi, copies)
-        if h == VG_AFTER:
-            for i in range(2):
-                group = vg_send.at[pl.ds(i * shared, shared)]
-                to_owner(i, [("vg", group, vg_in.at[owner_slot(i)])])
 
     @pl.when(is_owner)
     def _():
@@ -492,6 +499,29 @@
         base = oi * shared
         units = [(c, hh) for c in (1, 0) for hh in range(shared)]
         slots = {0: range(n_kv), 1: range(n_kv, 2 * n_kv - 1)}
+        wait_in("vg", vg_in)
+        near = {0: range(n_kv // 2), 1: range(n_kv // 2, n_kv - 1)}
+
+        def half_sum(c, head, i):
+            parts = [vg_in[k, head, i] for k in near[c]]
+            if c:
+                parts.append(vg_send[head, i])
+            total = unpack(parts[0])
+            for part in parts[1:]:
+                total = total + unpack(part)
+            return total
+
+        for c, hh in units:
+            for i in range(2):
+                swap_send[c, hh, i] = pack(half_sum(c, shared - base + hh, i))
+        for i in range(2):
+
+            @pl.when(oi == i)
+            def _():
+                where = {"kv": middle + 1 - i}
+                remote("swap", "swap", swap_send, swap_recv, where).start()
+
+        sums_of = {(c, hh, i): half_sum(c, base + hh, i) for c, hh in units for i in range(2)}
         wait_in("sc", sc_in)
         lines = {}
         for c in (0, 1):
@@ -500,21 +530,13 @@
         factor = lax.rsqrt(column_of(lines[1], shared) / D + RMS_EPS)
         cubed = factor * factor * factor
         weights = {u: column_of(lines[u[0]], u[1]) * cubed for u in units}
-        wait_in("vg", vg_in)
+        wait_in("swap", swap_recv)
         gates, news = {}, {}
         for c, hh in units:
-            parts = [[vg_in[k, hh, i] for k in slots[c]] for i in range(2)]
-            if c:
-                parts = [[vg_send[base + hh, i]] + parts[i] for i in range(2)]
-            both = []
-            for i in range(2):
-                total = unpack(parts[i][0])
-                for part in parts[i][1:]:
-                    total = total + unpack(part)
-                both.append(total)
+            both = [sums_of[c, hh, i] + unpack(swap_recv[c, hh, i]) for i in range(2)]
             news[c, hh] = weights[c, hh] * both[0]
-            both[1] = both[1] * factor
-            gates[c, hh] = both[1] / (1.0 + jnp.exp(-both[1]))
+            gate = both[1] * factor
+            gates[c, hh] = gate / (1.0 + jnp.exp(-gate))
         wait_in("ca", ca_in)
         totals = {}
         for c, hh in units:
@@ -556,11 +578,25 @@
             unpack(gt_buf[h // shared, h % shared]) * gn_gain_ref[:, cols]
         ).astype(BF16)
     gated = x_buf[...]
+
+    def o_send(part, core):
+        mine = o_buf.at[part, me_tp]
+        if core is None:
+            remote("o", f"o{part}", mine, mine, {"tp": tp_peer(1)}).start()
+        else:
+            for chip in range(n_tp // 2 - 1, 0, -1):
+                target = partner(first_core, 2 * chip, n_tp) + core
+                remote("o", f"o{part}", mine, mine, {"tp": target}).start()
+
     for part in range(2):
         width = depth // 2
         piece = jnp.dot(gated, wo[:, pl.ds(part * width, width)], preferred_element_type=F32)
         o_buf[part, me_tp] = pack(piece)
-        to_tp("o", f"o{part}", lambda target: o_buf.at[part, me_tp], o_buf.at[part, me_tp])
+        o_send(part, 0)
+    for part in range(2):
+        o_send(part, 1)
+    for part in range(2):
+        o_send(part, None)
     loads["fg"].wait()
     for part in range(2):
         wait_in(f"o{part}", o_buf.at[part, pl.ds(0, n_tp - 1)])
@@ -720,15 +756,19 @@
         @pl.when(jnp.logical_not((me_core == 1) & (me_kv == middle + i)))
         def _():
             group = pl.ds(i * shared, shared)
-            wait_out(f"vg{i}", vg_send.at[group])
             wait_out(f"ca{i}", ca_send.at[group])
             wait_out(f"sc{i}", sc_send.at[i])
             if rest:
                 wait_out(f"rest{i}", rest_send.at[i])
 
+    @pl.when(jnp.logical_not(is_owner))
+    def _():
+        wait_out("vg", vg_send)
+
     @pl.when(is_owner)
     def _():
         wait_out("gt", ca_in)
+        wait_out("swap", swap_send)
         if rest:
             wait_out("rhid", rest_hid)
 
@@ -798,7 +838,9 @@
         pltpu.VMEM((heads, rows, rows * span), F32),
         pltpu.VMEM((rows, wide), F32),
         pltpu.VMEM((heads, 2, *piece), BF16),
-        pltpu.VMEM((2 * n_kv - 1, shared, 2, *piece), BF16),
+        pltpu.VMEM((peers, heads, 2, *piece), BF16),
+        pltpu.VMEM((2, shared, 2, *piece), BF16),
+        pltpu.VMEM((2, shared, 2, *piece), BF16),
         pltpu.VMEM((heads, *piece), BF16),
         pltpu.VMEM((2 * n_kv - 1, shared, *piece), BF16),
         pltpu.VMEM((2, 1, LANES), F32),
@@ -823,7 +865,7 @@
         pltpu.VMEM((n_tp, 2 * rows, own_cols // 2), BF16),
         pltpu.SemaphoreType.DMA((len(small) + len(streamed),)),
         pltpu.SemaphoreType.DMA((17,)),
-        pltpu.SemaphoreType.DMA((13 + heads + 2 * n_full,)),
+        pltpu.SemaphoreType.DMA((14 + heads + 2 * n_full,)),
         pltpu.SemaphoreType.REGULAR,
     ]
     return pl.pallas_call(

time: 40.8 us -> 40.1 us (0.983)
  Pallas kernels: 40.1 us -> 39.4 us
    pallas_call x1, Pallas kernels: 40.1 us -> 39.4 us  [fused(): pl.pallas_call(functools.partial(layer_kernel, n_kv, n_tp), out_shape=plt...]
where the time goes in v5:
time: 40.1 us; the launch traced here: 40 us
  Pallas kernels  39.4 us (98%)
  local copies, waits for them, and re-layouts  0.6 us (1%)
    pallas_call x1, Pallas kernels, fused(): pl.pallas_call(functools.partial(layer_kernel, n_kv, n_tp), out_shape=plt...  39.4 us

profile of v5, /device:TPU:0, one launch (start us, length us, event | category | flops | bytes accessed | tf_op | source)
XLA Modules:
  0.0 40.0 jit_solution(2261376919858227332)
XLA Ops:
  0.0 39.4 %shard_map.154 = bf16[24,256]{1,0:T(8,128)(2,1)S(1)} custom-call(bf16[24,256]{1,0:T(8,128)(2,1)} %tokens_hbm.1, s32[24]{0:T(128)} %lengths_hbm.1, f32[1,1024]{1,0:T(1,128)} %bitcast.3, f32[4]{0:T(128)} %log_decay_hbm.1, f32[1,1024]{1,0:T(1,128)} %bitcast.4, f32[1,1024]{1,0:T(1,128)} %bitcast.5, bf16[1024,1024]{1,0:T(8,128)(2,1)} %wq_hbm.1, ...), custom_call_target="tpu_custom_call" | custom-call | tf_op jit(solution)/shard_map/pallas_call | solution.py:871
  39.4 0.6 %copy.18 = bf16[24,256]{1,0:T(8,128)(2,1)} copy(bf16[24,256]{1,0:T(8,128)(2,1)S(1)} %shard_map.154) | data formatting | bytes 24576

commit v6 on v5

--- a/solution.py
+++ b/solution.py
@@ -258,6 +258,9 @@
     first_core = me_tp - me_core
     is_middle = (me_kv >= middle) & (me_kv < middle + 2)
     is_owner = (me_core == 1) & is_middle
+    side = jnp.where(me_kv > middle, 1, 0)
+    far_group = pl.ds((1 - side) * shared, shared)
+    near_group = pl.ds(side * shared, shared)
 
     def kv_peer(j):
         return partner(me_kv, j, n_kv)
@@ -307,7 +310,7 @@
     names += [f"{kind}{i}" for kind in ("ca", "sc", "rest") for i in range(2)]
     names += ["vg", "swap"]
     out_slot = {name: i for i, name in enumerate(names)}
-    names = ["tok", "vg", "swap", "ca", "sc", "gt0", "gt1", "o0", "o1", "sqm", "d"]
+    names = ["tok", "vgf", "vgn", "swap", "ca", "sc", "gt0", "gt1", "o0", "o1", "sqm", "d"]
     names += [f"q{h}" for h in range(heads)] + ["rest", "rhid0", "rhid1"]
     names += [f"{kind}{i}" for kind in ("gu", "hid") for i in range(n_full)]
     in_slot = {name: i for i, name in enumerate(names)}
@@ -417,17 +420,42 @@
 
     x = x_buf[...]
     loads["wq"].wait()
-    for pair in range(heads // 2):
-        q_own = jnp.dot(x, wq[:, pl.ds(pair * 2 * DK, 2 * DK)], preferred_element_type=F32)
-        for i in range(2):
-            h = pair * 2 + i
-            piece = q_own[:, i * DK : (i + 1) * DK]
-            q_send[h] = pack(piece)
-            q_full[:, pl.ds(h * DK, DK)] = piece
-            for j in kv_order:
-                remote(
-                    "q", f"q{h}", q_send.at[h], q_recv.at[h, j - 1], {"kv": kv_peer(j)}
+
+    def head_at(place):
+        return ((1 - side) if place < shared else side) * shared + place % shared
+
+    def head_cols(h):
+        return pl.ds(pl.multiple_of(h * DK, DK), DK)
+
+    def q_slot(h):
+        return recv_sem.at[in_slot["q0"] + h]
+
+    def send_q(group, peers):
+        for i in range(shared):
+            h = group * shared + i
+            for j in peers:
+                pltpu.make_async_remote_copy(
+                    src_ref=q_send.at[h],
+                    dst_ref=q_recv.at[h, j - 1],
+                    send_sem=send_sem.at[out_slot["q"]],
+                    recv_sem=q_slot(h),
+                    device_id={"kv": kv_peer(j)},
+                    device_id_type=pl.DeviceIdType.MESH,
                 ).start()
+
+    across = [j for j in kv_order if j >= n_kv // 2]
+    beside = [j for j in kv_order if j < n_kv // 2]
+    for group in (side, 1 - side):
+        cols = pl.ds(pl.multiple_of(group * shared * DK, DK), shared * DK)
+        q_own = jnp.dot(x, wq[:, cols], preferred_element_type=F32)
+        q_full[:, cols] = q_own
+        for i in range(shared):
+            q_send[group * shared + i] = pack(q_own[:, i * DK : (i + 1) * DK])
+        if group is side:
+            send_q(side, across)
+    send_q(1 - side, beside)
+    send_q(1 - side, across)
+    send_q(side, beside)
     for name in ("wo", "wfg", "wfu", "wfd"):
         loads[name].start()
 
@@ -438,22 +466,26 @@
             part = jnp.dot(x, weight[:, pl.ds(pair * 2 * DK, 2 * DK)], preferred_element_type=F32)
             for k in range(2):
                 vg_send[pair * 2 + k, i] = pack(part[:, k * DK : (k + 1) * DK])
-    side = jnp.where(me_kv > middle, 1, 0)
     away = jnp.where(me_kv > middle, me_kv - middle - 1, middle - me_kv)
 
     @pl.when(jnp.logical_not(is_owner))
     def _():
         slot = jnp.where(me_core == 0, away, n_kv // 2 - 1 + away)
         where = {"kv": middle + side, "tp": first_core + 1}
-        remote("vg", "vg", vg_send, vg_in.at[slot], where).start()
+        for into, group in (("vgf", far_group), ("vgn", near_group)):
+            remote("vg", into, vg_send.at[group], vg_in.at[slot, group], where).start()
 
     key_own[...] = jnp.dot(x, wk[...], preferred_element_type=F32)
 
     loads["kc"].wait()
     loads["vc"].wait()
 
+    def apart_from(oi):
+        both = [partner(me_kv, middle + i, n_kv) for i in range(2)]
+        return jnp.where(oi == 1, both[1], both[0])
+
     def owner_slot(oi):
-        apart = partner(me_kv, middle + oi, n_kv)
+        apart = apart_from(oi)
         return jnp.where(me_core == 0, me_kv, n_kv - 1 + apart)
 
     def to_owner(oi, copies):
@@ -464,9 +496,17 @@
                 remote(f"{kind}{oi}", kind, src, dst, where).start()
 
     own_scores = []
-    for h in range(heads):
-        cols = pl.ds(h * DK, DK)
-        wait_in(f"q{h}", q_recv.at[h])
+    for place in range(heads):
+        h = head_at(place)
+        cols = head_cols(h)
+        pltpu.make_async_remote_copy(
+            src_ref=q_recv.at[h],
+            dst_ref=q_recv.at[h],
+            send_sem=send_sem.at[out_slot["q"]],
+            recv_sem=q_slot(h),
+            device_id={"kv": kv_peer(1)},
+            device_id_type=pl.DeviceIdType.MESH,
+        ).wait_recv()
         query = q_full[:, cols]
         for j in kv_order:
             query = query + unpack(q_recv[h, j - 1])
@@ -486,12 +526,22 @@
         own_scores.append(
             jnp.sum(query[:, :half] * front + query[:, half:] * back, axis=1, keepdims=True)
         )
-        oi, hh = h // shared, h % shared
-        copies = [("ca", ca_send.at[h], ca_in.at[owner_slot(oi), hh])]
+        near, hh = place // shared, place % shared
+        oi = side if near else 1 - side
+        copies = [(f"ca{near}", "ca", ca_send.at[h], ca_in.at[owner_slot(oi), hh])]
         if hh == shared - 1:
-            sc_send[oi] = lanes_of(own_scores[oi * shared :] + [squares])
-            copies.append(("sc", sc_send.at[oi], sc_in.at[owner_slot(oi)]))
-        to_owner(oi, copies)
+            sc_send[oi] = lanes_of(own_scores[near * shared :] + [squares])
+            copies.append((f"sc{near}", "sc", sc_send.at[oi], sc_in.at[owner_slot(oi)]))
+
+        def send_all():
+            for out, into, src, dst in copies:
+                where = {"kv": middle + oi, "tp": first_core + 1}
+                remote(out, into, src, dst, where).start()
+
+        if near:
+            pl.when(jnp.logical_not(is_owner))(send_all)
+        else:
+            send_all()
 
     @pl.when(is_owner)
     def _():
@@ -499,7 +549,7 @@
         base = oi * shared
         units = [(c, hh) for c in (1, 0) for hh in range(shared)]
         slots = {0: range(n_kv), 1: range(n_kv, 2 * n_kv - 1)}
-        wait_in("vg", vg_in)
+        wait_in("vgf", vg_in.at[:, pl.ds(0, shared)])
         near = {0: range(n_kv // 2), 1: range(n_kv // 2, n_kv - 1)}
 
         def half_sum(c, head, i):
@@ -521,6 +571,7 @@
                 where = {"kv": middle + 1 - i}
                 remote("swap", "swap", swap_send, swap_recv, where).start()
 
+        wait_in("vgn", vg_in.at[:, pl.ds(0, shared)])
         sums_of = {(c, hh, i): half_sum(c, base + hh, i) for c, hh in units for i in range(2)}
         wait_in("sc", sc_in)
         lines = {}
@@ -755,11 +806,16 @@
 
         @pl.when(jnp.logical_not((me_core == 1) & (me_kv == middle + i)))
         def _():
-            group = pl.ds(i * shared, shared)
-            wait_out(f"ca{i}", ca_send.at[group])
-            wait_out(f"sc{i}", sc_send.at[i])
             if rest:
                 wait_out(f"rest{i}", rest_send.at[i])
+
+    wait_out("ca0", ca_send.at[far_group])
+    wait_out("sc0", sc_send.at[0])
+
+    @pl.when(jnp.logical_not(is_owner))
+    def _():
+        wait_out("ca1", ca_send.at[near_group])
+        wait_out("sc1", sc_send.at[0])
 
     @pl.when(jnp.logical_not(is_owner))
     def _():
@@ -865,7 +921,7 @@
         pltpu.VMEM((n_tp, 2 * rows, own_cols // 2), BF16),
         pltpu.SemaphoreType.DMA((len(small) + len(streamed),)),
         pltpu.SemaphoreType.DMA((17,)),
-        pltpu.SemaphoreType.DMA((14 + heads + 2 * n_full,)),
+        pltpu.SemaphoreType.DMA((15 + heads + 2 * n_full,)),
         pltpu.SemaphoreType.REGULAR,
     ]
     return pl.pallas_call(

time: 40.1 us -> 39.2 us (0.978)
  Pallas kernels: 39.4 us -> 38.4 us
    pallas_call x1, Pallas kernels: 39.4 us -> 38.4 us  [fused(): pl.pallas_call(functools.partial(layer_kernel, n_kv, n_tp), out_shape=plt...]
where the time goes in v6:
time: 39.2 us; the launch traced here: 39 us
  Pallas kernels  38.4 us (98%)
  local copies, waits for them, and re-layouts  0.6 us (2%)
    pallas_call x1, Pallas kernels, fused(): pl.pallas_call(functools.partial(layer_kernel, n_kv, n_tp), out_shape=plt...  38.4 us

profile of v6, /device:TPU:0, one launch (start us, length us, event | category | flops | bytes accessed | tf_op | source)
XLA Modules:
  0.0 39.0 jit_solution(6179708827287590358)
XLA Ops:
  0.0 38.4 %shard_map.154 = bf16[24,256]{1,0:T(8,128)(2,1)S(1)} custom-call(bf16[24,256]{1,0:T(8,128)(2,1)} %tokens_hbm.1, s32[24]{0:T(128)} %lengths_hbm.1, f32[1,1024]{1,0:T(1,128)} %bitcast.3, f32[4]{0:T(128)} %log_decay_hbm.1, f32[1,1024]{1,0:T(1,128)} %bitcast.4, f32[1,1024]{1,0:T(1,128)} %bitcast.5, bf16[1024,1024]{1,0:T(8,128)(2,1)} %wq_hbm.1, ...), custom_call_target="tpu_custom_call" | custom-call | tf_op jit(solution)/shard_map/pallas_call | solution.py:927
  38.4 0.6 %copy.18 = bf16[24,256]{1,0:T(8,128)(2,1)} copy(bf16[24,256]{1,0:T(8,128)(2,1)S(1)} %shard_map.154) | data formatting | bytes 24576

commit v7 on v6

--- a/solution.py
+++ b/solution.py
@@ -443,7 +443,7 @@
                     device_id_type=pl.DeviceIdType.MESH,
                 ).start()
 
-    across = [j for j in kv_order if j >= n_kv // 2]
+    across = [j for j in range(1, n_kv) if j >= n_kv // 2]
     beside = [j for j in kv_order if j < n_kv // 2]
     for group in (side, 1 - side):
         cols = pl.ds(pl.multiple_of(group * shared * DK, DK), shared * DK)
@@ -607,7 +607,7 @@
             if c:
                 gt_buf[oi, hh] = result
         for c in (0, 1):
-            for j in kv_order + ((0,) if c == 0 else ()):
+            for j in (3, 1, 2) + ((0,) if c == 0 else ()):
                 where = {"kv": kv_peer(j) if j else me_kv, "tp": first_core + c}
                 for i in range(2):
 
@@ -722,7 +722,7 @@
                 total = total + unpack(gu_recv[s, j - 1, i])
             both.append(total)
         hid_send[s] = pack(activate(*both))
-        for j in kv_order:
+        for j in (2, 3, 1):
             remote(
                 "hid", f"hid{s}", hid_send.at[s], hid_recv.at[s, j - 1], {"kv": kv_peer(j)}
             ).start()

time: 39.2 us -> 38.9 us (level)
  no operation moved by 1% of the time
where the time goes in v7:
time: 38.9 us; the launch traced here: 38.8 us
  Pallas kernels  38.2 us (98%)
  local copies, waits for them, and re-layouts  0.6 us (2%)
    pallas_call x1, Pallas kernels, fused(): pl.pallas_call(functools.partial(layer_kernel, n_kv, n_tp), out_shape=plt...  38.2 us

profile of v7, /device:TPU:0, one launch (start us, length us, event | category | flops | bytes accessed | tf_op | source)
XLA Modules:
  0.0 38.8 jit_solution(7815594491636560094)
XLA Ops:
  0.0 38.2 %shard_map.154 = bf16[24,256]{1,0:T(8,128)(2,1)S(1)} custom-call(bf16[24,256]{1,0:T(8,128)(2,1)} %tokens_hbm.1, s32[24]{0:T(128)} %lengths_hbm.1, f32[1,1024]{1,0:T(1,128)} %bitcast.3, f32[4]{0:T(128)} %log_decay_hbm.1, f32[1,1024]{1,0:T(1,128)} %bitcast.4, f32[1,1024]{1,0:T(1,128)} %bitcast.5, bf16[1024,1024]{1,0:T(8,128)(2,1)} %wq_hbm.1, ...), custom_call_target="tpu_custom_call" | custom-call | tf_op jit(solution)/shard_map/pallas_call | solution.py:927
  38.2 0.6 %copy.18 = bf16[24,256]{1,0:T(8,128)(2,1)} copy(bf16[24,256]{1,0:T(8,128)(2,1)S(1)} %shard_map.154) | data formatting | bytes 24576

commit v8 on v7

--- a/solution.py
+++ b/solution.py
@@ -186,14 +186,10 @@
     wfd_hbm,
     out_ref,
     wq,
-    wk,
-    wv,
-    wg,
-    kc,
-    vc,
+    wkvg,
+    caches,
     wo,
-    wfg,
-    wfu,
+    wgu,
     wfd,
     tokens_ref,
     lengths_ref,
@@ -240,6 +236,9 @@
     recv_sem,
     go_sem,
 ):
+    wk, wv, wg = [wkvg.at[i] for i in range(3)]
+    kc, vc = [caches.at[i] for i in range(2)]
+    wfg, wfu = [wgu.at[i] for i in range(2)]
     rows, own_cols = tokens_ref.shape
     depth, wide = wq.shape
     span = kc.shape[1]
@@ -283,7 +282,11 @@
                 barrier, inc=1, device_id={"kv": k}, device_id_type=pl.DeviceIdType.MESH
             )
 
-    loads = {}
+    loads, load_slot = {}, {}
+
+    def wait_group(name, ref):
+        pltpu.make_async_copy(ref, ref, load_sem.at[load_slot[name]]).wait()
+
     for slot, (name, src, dst) in enumerate(
         (
             ("tok", tokens_hbm, tokens_ref),
@@ -304,7 +307,9 @@
             ("wfd", wfd_hbm, wfd),
         )
     ):
-        loads[name] = pltpu.make_async_copy(src, dst, load_sem.at[slot])
+        shared_slot = {"vc": "kc", "wv": "wk", "wg": "wk", "wfu": "wfg"}.get(name, name)
+        load_slot.setdefault(shared_slot, len(load_slot))
+        loads[name] = pltpu.make_async_copy(src, dst, load_sem.at[load_slot[shared_slot]])
 
     names = ["tok", "q", "o", "sqm", "gu", "hid", "d", "gt", "rhid"]
     names += [f"{kind}{i}" for kind in ("ca", "sc", "rest") for i in range(2)]
@@ -459,8 +464,7 @@
     for name in ("wo", "wfg", "wfu", "wfd"):
         loads[name].start()
 
-    for name in ("wk", "wv", "wg"):
-        loads[name].wait()
+    wait_group("wk", wkvg)
     for i, weight in enumerate((wv, wg)):
         for pair in range(heads // 2):
             part = jnp.dot(x, weight[:, pl.ds(pair * 2 * DK, 2 * DK)], preferred_element_type=F32)
@@ -477,8 +481,7 @@
 
     key_own[...] = jnp.dot(x, wk[...], preferred_element_type=F32)
 
-    loads["kc"].wait()
-    loads["vc"].wait()
+    wait_group("kc", caches)
 
     def apart_from(oi):
         both = [partner(me_kv, middle + i, n_kv) for i in range(2)]
@@ -672,8 +675,7 @@
         remote("sqm", "sqm", sqm_send, sqm_recv.at[j - 1], {"kv": kv_peer(j)}).start()
 
     x = x_buf[...]
-    loads["wfg"].wait()
-    loads["wfu"].wait()
+    wait_group("wfg", wgu)
 
     def stage_start(s, index):
         return pl.multiple_of((s * n_kv + index) * win, win)
@@ -880,7 +882,15 @@
         w_ffn_up,
         w_ffn_down,
     )
-    scratch = [pltpu.VMEM(a.shape, a.dtype) for a in streamed] + [
+    resident = [
+        w_query.shape,
+        (3, *w_key.shape),
+        (2, *key_cache.shape),
+        w_out.shape,
+        (2, *w_ffn_gate.shape),
+        w_ffn_down.shape,
+    ]
+    scratch = [pltpu.VMEM(shape, BF16) for shape in resident] + [
         (pltpu.SMEM if a.ndim == 1 else pltpu.VMEM)(a.shape, a.dtype) for a in small
     ]
     piece = (2 * rows, DK // 2)
@@ -919,7 +929,7 @@
         pltpu.VMEM((rows, depth), F32),
         pltpu.VMEM((n_tp, 2 * rows, own_cols // 2), BF16),
         pltpu.VMEM((n_tp, 2 * rows, own_cols // 2), BF16),
-        pltpu.SemaphoreType.DMA((len(small) + len(streamed),)),
+        pltpu.SemaphoreType.DMA((len(small) + len(resident),)),
         pltpu.SemaphoreType.DMA((17,)),
         pltpu.SemaphoreType.DMA((15 + heads + 2 * n_full,)),
         pltpu.SemaphoreType.REGULAR,

time: 38.9 us -> 38.9 us (level)
  no operation moved by 1% of the time
where the time goes in v8:
time: 38.9 us; the launch traced here: 38.7 us
  Pallas kernels  38.1 us (98%)
  local copies, waits for them, and re-layouts  0.6 us (2%)
    pallas_call x1, Pallas kernels, fused(): pl.pallas_call(functools.partial(layer_kernel, n_kv, n_tp), out_shape=plt...  38.1 us

profile of v8, /device:TPU:0, one launch (start us, length us, event | category | flops | bytes accessed | tf_op | source)
XLA Modules:
  0.0 38.7 jit_solution(10700784526350604310)
XLA Ops:
  0.0 38.1 %shard_map.154 = bf16[24,256]{1,0:T(8,128)(2,1)S(1)} custom-call(bf16[24,256]{1,0:T(8,128)(2,1)} %tokens_hbm.1, s32[24]{0:T(128)} %lengths_hbm.1, f32[1,1024]{1,0:T(1,128)} %bitcast.3, f32[4]{0:T(128)} %log_decay_hbm.1, f32[1,1024]{1,0:T(1,128)} %bitcast.4, f32[1,1024]{1,0:T(1,128)} %bitcast.5, bf16[1024,1024]{1,0:T(8,128)(2,1)} %wq_hbm.1, ...), custom_call_target="tpu_custom_call" | custom-call | tf_op jit(solution)/shard_map/pallas_call | solution.py:937
  38.1 0.6 %copy.18 = bf16[24,256]{1,0:T(8,128)(2,1)} copy(bf16[24,256]{1,0:T(8,128)(2,1)S(1)} %shard_map.154) | data formatting | bytes 24576
